TPU v7x, 512 devices: a 4x2x32 block of a 4x8x32 slice. The times are simulated.
512 devices in a mesh: grp: 2 (over y), sp: 64 (over z, core), tp: 4 (over x).
Axes of the slice: x: 4, y: 2, z: 32, core: 2. Of those that a mesh axis runs over, the one named last changes fastest.
The devices are a block of a 4x8x32 slice.
Arguments:
- tokens: bfloat16 [32768, 2048], P(('grp', 'sp'), 'tp'), parts along dimension 0, may hold values from -6 to 6
- norm_gain: float32 [2048], replicated, may hold values from 0.1 to 1.9
- ret_query_weight: bfloat16 [2048, 256], P('sp', 'tp'), may hold values from -0.125 to 0.125
- ret_key_weight: bfloat16 [2048, 256], P('sp', 'tp'), may hold values from -0.125 to 0.125
- ret_value_weight: bfloat16 [2048, 512], P('sp', 'tp'), may hold values from -0.125 to 0.125
- fox_query_weight: bfloat16 [2048, 512], P('sp', 'tp'), may hold values from -8 to 8
- fox_key_weight: bfloat16 [2048, 512], P('sp', 'tp'), may hold values from -0.125 to 0.125
- fox_value_weight: bfloat16 [2048, 512], P('sp', 'tp'), may hold values from -0.125 to 0.125
- ret_decay: float32 [8], P('tp'), may hold values from -1 to 0, as said below
- ret_state: float32 [16, 32, 64], P(('grp', 'tp')), parts along dimension 0, may hold values from -256 to 256
- head_norm_gain: float32 [512], P('tp'), may hold values from 0.1 to 1.9
- fox_gates: float32 [32768, 8], P('grp', 'tp'), parts along dimension 0, may hold values from -49152 to 0, as said below
- ret_out_weight: bfloat16 [512, 2048], P('tp', 'sp'), may hold values from -0.1875 to 0.1875
- fox_out_weight: bfloat16 [512, 2048], P('tp', 'sp'), may hold values from -1 to 1
Outputs:
- mixed: bfloat16 [32768, 2048], P(('grp', 'sp', 'tp')), parts along dimension 0
There are 2 independent parts, one for each index of `grp`. A program takes and returns all parts, laid end to end along the dimension named above; an argument that names none is the same for every part. Nothing has to cross between parts.
Inputs may be any that keep to these rules, and one draw needn't show every extreme that they name: `ret_decay`: each head's log decay is negative. `fox_gates`: along the positions each head's column never rises.
All inputs are finite; a program needn't handle non-finite values.
Results may differ from a plain program's by a relative error of at most 0.015.
The roundings to bfloat16 on the way count: a program that leaves them out, or rounds other values in their place, can miss the bound.
Values may be sent and summed in bfloat16 or wider, within the bound.
A program may use at most 64 MiB of HBM per device.

v0:
```python
import jax
import jax.numpy as jnp
from jax import lax
from jax.sharding import Mesh
from jax.sharding import PartitionSpec as P

SP = ("sp_0", "sp_1")
GRP_SP = ("grp", "sp_0", "sp_1")
GRP_SP_TP = ("grp", "sp_0", "sp_1", "tp")


epsilon = 1e-06


def in_order(blocks, dim):
    shape = list(blocks.shape[1:])
    shape[dim] *= blocks.shape[0]
    return jnp.moveaxis(blocks, 0, dim).reshape(shape)


def from_everyone(array, axis):
    count = lax.axis_size(axis)
    return lax.all_to_all(
        jnp.broadcast_to(array[None], (count, *array.shape)), axis, 0, 0, tiled=True
    )


def collect_2(array, axis, dim):
    return in_order(from_everyone(array, axis), dim)


def sent_together(arrays, axis, dim, along):
    widths = [a.shape[along] for a in arrays]
    both = jnp.concatenate(arrays, axis=along)
    result = lax.all_gather(both, axis, axis=dim, tiled=True)
    return tuple(jnp.split(result, [sum(widths[:k]) for k in range(1, len(widths))], axis=along))


def all_blocks(array, axes, order):
    blocks = array
    for k in order:
        blocks = lax.all_gather(blocks, axes[k])
    done = order[::-1]
    back = [done.index(k) for k in range(len(axes))]
    blocks = blocks.transpose(*back, *range(len(axes), blocks.ndim))
    return blocks.reshape(-1, *array.shape)


def whole_of(array, axes, order, dim):
    return in_order(all_blocks(array, axes, order), dim)


def rows_first(arrays, axis, dims):
    turned = [jnp.moveaxis(a, dim, 0) for a, dim in zip(arrays, dims)]
    both = jnp.concatenate([t.reshape(len(t), -1) for t in turned], axis=1)
    result, at, gathered = (lax.all_gather(both, axis, axis=0, tiled=True), 0, [])
    for t, dim in zip(turned, dims):
        piece = result[:, at : at + t[0].size].reshape(-1, *t.shape[1:])
        gathered.append(jnp.moveaxis(piece, 0, dim))
        at += t[0].size
    return tuple(gathered)


def in_blocks(array, dim, count):
    before, after = (array.shape[:dim], array.shape[dim + 1 :])
    return jnp.moveaxis(array.reshape(*before, count, -1, *after), dim, 0)


def summed_on_arrival(array, axis, dim):
    blocks = in_blocks(array, dim, lax.axis_size(axis))
    arrived = lax.all_to_all(blocks, axis, split_axis=0, concat_axis=0, tiled=True)
    return arrived.astype(jnp.float32).sum(axis=0)


def head_group_norm(joined_output, norm_gains):
    center = joined_output - jnp.mean(joined_output, axis=-1, keepdims=True)
    spread = jnp.mean(center * center, axis=-1, keepdims=True)
    normal = (
        center
        * lax.rsqrt(spread + epsilon)
        * norm_gains.reshape(joined_output.shape[1], joined_output.shape[2])
    )
    return normal.reshape(joined_output.shape[0], -1).astype(jnp.bfloat16)


def softmax_update(
    current,
    query_heads,
    query_gates,
    query_pos,
    key_block,
    value_block,
    gate_block,
    key_pos,
    score_scale,
):
    top_now, total_now, weighted = current
    logits = (
        jnp.einsum("qhd,khd->hqk", query_heads, key_block, preferred_element_type=jnp.float32)
        * score_scale
    )
    logits = logits + query_gates[:, :, None] - gate_block[:, None, :]
    logits = jnp.where(key_pos[None, None, :] <= query_pos[None, :, None], logits, -jnp.inf)
    top_new = jnp.maximum(top_now, jnp.max(logits, axis=-1))
    weights_new = jnp.exp(logits - top_new[:, :, None])
    rescale = jnp.exp(top_now - top_new)
    total_new = total_now * rescale + jnp.sum(weights_new, axis=-1)
    weighted_new = weighted * rescale[:, :, None] + jnp.einsum(
        "hqk,khd->hqd",
        weights_new.astype(jnp.bfloat16),
        value_block,
        preferred_element_type=jnp.float32,
    )
    return (top_new, total_new, weighted_new)


def local(
    tokens,
    norm_gain,
    ret_query_weight,
    ret_key_weight,
    ret_value_weight,
    fox_query_weight,
    fox_key_weight,
    fox_value_weight,
    ret_decay,
    ret_state,
    head_norm_gain,
    fox_gates,
    ret_out_weight,
    fox_out_weight,
):
    sequence_length = tokens.shape[0]
    gathered = collect_2(tokens, "tp", 1)
    widened = gathered.astype(jnp.float32)
    normed = (
        widened
        * lax.rsqrt(jnp.mean(widened * widened, axis=-1, keepdims=True) + epsilon)
        * norm_gain
    ).astype(jnp.bfloat16)
    portions = sent_together(
        (
            ret_query_weight,
            ret_key_weight,
            ret_value_weight,
            fox_query_weight,
            fox_key_weight,
            fox_value_weight,
        ),
        SP,
        0,
        1,
    )
    sums = tuple(
        (jnp.dot(normed, portion, preferred_element_type=jnp.float32) for portion in portions)
    )
    ret_query, ret_key, ret_value, fox_query, fox_key, fox_value = [
        result.astype(jnp.bfloat16) for result in sums
    ]
    ret_heads = ret_decay.shape[0]
    key_size = ret_query.shape[1] // ret_heads
    value_size = ret_value.shape[1] // ret_heads
    place = lax.axis_index(SP)
    offset = place * sequence_length
    queries = ret_query.astype(jnp.float32).reshape(sequence_length, ret_heads, key_size)
    keys_local = ret_key.astype(jnp.float32).reshape(
        sequence_length, ret_heads, key_size
    ) * key_size ** (-0.5)
    values_local = ret_value.astype(jnp.float32).reshape(sequence_length, ret_heads, value_size)
    positions = jnp.arange(sequence_length, dtype=jnp.float32)
    spread = positions[:, None] - positions[None, :]
    within = jnp.where(
        spread[None] >= 0, jnp.exp(jnp.maximum(spread, 0.0)[None] * ret_decay[:, None, None]), 0.0
    )
    leading = jnp.exp((positions + 1.0)[:, None] * ret_decay[None, :])
    trailing = jnp.exp((sequence_length - 1.0 - positions)[:, None] * ret_decay[None, :])
    scores = jnp.einsum("ihd,jhd->hij", queries, keys_local) * within
    inner_value = jnp.einsum("hij,jhe->ihe", scores, values_local)
    summary = jnp.einsum("jhd,jhe->hde", keys_local * trailing[:, :, None], values_local)
    portion = whole_of(summary[None], SP, (0, 1), 0)
    shard_ids = jnp.arange(portion.shape[0], dtype=jnp.int32)
    distance = jnp.maximum(place - shard_ids - 1, 0).astype(jnp.float32) * sequence_length
    weight = jnp.where(
        (shard_ids < place)[:, None], jnp.exp(distance[:, None] * ret_decay[None, :]), 0.0
    )
    before = jnp.einsum("sh,shde->hde", weight, portion)
    entering = jnp.exp(offset.astype(jnp.float32) * ret_decay)[:, None, None] * ret_state + before
    carried_state = jnp.einsum("ihd,hde->ihe", queries, entering) * leading[:, :, None]
    retention_mixed = head_group_norm(inner_value + carried_state, head_norm_gain)
    fox_heads = fox_gates.shape[1]
    head_size = fox_query.shape[1] // fox_heads
    score_scale = head_size ** (-0.5)
    starting = (
        jnp.full((fox_heads, sequence_length), -1e30, jnp.float32),
        jnp.zeros((fox_heads, sequence_length), jnp.float32),
        jnp.zeros((fox_heads, sequence_length, head_size), jnp.float32),
    )
    query_heads = fox_query.reshape(sequence_length, fox_heads, head_size)
    own_gates = lax.dynamic_slice_in_dim(fox_gates, offset, sequence_length, 0).T
    query_pos = offset + jnp.arange(sequence_length, dtype=jnp.int32)
    last_query = offset + sequence_length - 1

    def attend(running, portion, first_key):
        key_rows, value_rows = portion
        count = key_rows.shape[0]
        block_rows = next(
            (candidate for candidate in (2048, 1024, 512) if count % candidate == 0), count
        )

        def advance(state_now, number):
            key_start = first_key + number * block_rows

            def compute(current):
                key_block = lax.dynamic_slice_in_dim(
                    key_rows, number * block_rows, block_rows, 0
                ).reshape(block_rows, fox_heads, head_size)
                value_block = lax.dynamic_slice_in_dim(
                    value_rows, number * block_rows, block_rows, 0
                ).reshape(block_rows, fox_heads, head_size)
                gate_block = lax.dynamic_slice_in_dim(fox_gates, key_start, block_rows, 0).T
                key_pos = key_start + jnp.arange(block_rows, dtype=jnp.int32)
                return softmax_update(
                    current,
                    query_heads,
                    own_gates,
                    query_pos,
                    key_block,
                    value_block,
                    gate_block,
                    key_pos,
                    score_scale,
                )

            def unchanged(current):
                return current

            return (lax.cond(key_start <= last_query, compute, unchanged, state_now), None)

        finished, _ = lax.scan(advance, running, jnp.arange(count // block_rows, dtype=jnp.int32))
        return finished

    top_final, total_final, weighted_final = attend(
        starting, sent_together((fox_key, fox_value), SP, 0, 1), jnp.int32(0)
    )
    fox_mix = (
        jnp.transpose(weighted_final / total_final[:, :, None], (1, 0, 2))
        .reshape(sequence_length, fox_heads * head_size)
        .astype(jnp.bfloat16)
    )
    ret_full, fox_full = rows_first((ret_out_weight, fox_out_weight), SP, (1, 1))
    mixed = summed_on_arrival(
        (
            jnp.dot(retention_mixed, ret_full, preferred_element_type=jnp.float32)
            + jnp.dot(fox_mix, fox_full, preferred_element_type=jnp.float32)
        ).astype(jnp.bfloat16),
        "tp",
        0,
    )
    return mixed.astype(jnp.bfloat16)


def solution(mesh):
    torus = Mesh(
        mesh.devices.reshape(mesh.shape["grp"], 32, 2, mesh.shape["tp"]),
        ("grp", "sp_0", "sp_1", "tp"),
    )
    return jax.shard_map(
        local,
        mesh=torus,
        in_specs=(
            P(GRP_SP, "tp"),
            P(),
            P(SP, "tp"),
            P(SP, "tp"),
            P(SP, "tp"),
            P(SP, "tp"),
            P(SP, "tp"),
            P(SP, "tp"),
            P("tp"),
            P(("grp", "tp"), None, None),
            P("tp"),
            P("grp", "tp"),
            P("tp", SP),
            P("tp", SP),
        ),
        out_specs=P(GRP_SP_TP, None),
        check_vma=False,
    )
```

profile of v0, /device:TPU:1888, one launch (start us, length us, event | category | flops | bytes accessed | tf_op | source)
XLA Modules:
  0.0 498.8 jit_solution(9401134259431210037)
XLA Ops:
  6.6 1.5 concatenate.9
  10.3 4.6 all-to-all-start
  15.7 14.3 %all-to-all-done = bf16[4,256,512]{1,2,0:T(8,128)(2,1)S(1)} async-done(((bf16[4,256,512]{1,2,0:T(8,128)(2,1)}), bf16[4,256,512]{1,2,0:T(8,128)(2,1)S(1)}, u32[]{:S(2)}, u32[]{:S(2)}) %all-to-all-start) | async-done | bytes 1048608 | tf_op jit(solution)/shard_map/all_to_all | solution.py:23
  30.7 98.4 %all-gather.6.cloned.1.call-done = bf16[2048,640]{1,0:T(8,128)(2,1)} async-done(((bf16[32,640]{1,0:T(8,128)(2,1)}), bf16[2048,640]{1,0:T(8,128)(2,1)}) %all-gather.6.cloned.1.call-update) | async-done | bytes 2621456 | tf_op jit(solution)/shard_map/all_gather | solution.py:35
  133.8 1.6 convolution_convert_fusion.4
  137.0 55.0 %all-gather = bf16[64,32,64]{2,1,0:T(8,128)(2,1)S(1)} all-gather(bf16[2,32,64]{2,1,0:T(8,128)(2,1)S(1)} %fusion.37), channel_id=2, replica_groups=mesh['grp'=2,'sp_0'=32,'sp_1'=2,'tp'=4] {'sp_0'}, dimensions={0}, use_global_device_ids=true | all-gather | bytes 270336 | tf_op jit(solution)/shard_map/all_gather | solution.py:42
  192.1 2.6 all-gather.1
  199.1 57.8 %all-gather.8.cloned.1.call-done = bf16[2048,256]{1,0:T(8,128)(2,1)} async-done(((bf16[32,256]{1,0:T(8,128)(2,1)}), bf16[2048,256]{1,0:T(8,128)(2,1)}) %all-gather.8.cloned.1.call-update) | async-done | bytes 1048592 | tf_op jit(solution)/shard_map/all_gather | solution.py:56
  256.9 1.5 fusion.23
  258.4 148.5 %all-gather.10.cloned.1.call-done = bf16[16384,256]{0,1:T(8,128)(2,1)} async-done(((bf16[256,256]{0,1:T(8,128)(2,1)}), bf16[16384,256]{0,1:T(8,128)(2,1)}) %all-gather.10.cloned.1.call-update) | async-done | bytes 8388624 | tf_op jit(solution)/shard_map/all_gather | solution.py:35
  406.9 5.8 %fusion.48 = (bf16[16384,128]{0,1:T(8,128)(2,1)}, bf16[16384,128]{0,1:T(8,128)(2,1)}) fusion(bf16[16384,256]{0,1:T(8,128)(2,1)} %all-gather.10.cloned.1.call-done), kind=kLoop, calls=%fused_computation.83 | loop fusion | bytes 16777216 | tf_op jit(solution)/shard_map/split | solution.py:36
  412.7 58.6 %while.15 = (s32[]{:T(128)}, f32[2,256]{1,0:T(2,128)S(1)}, f32[2,256]{1,0:T(2,128)S(1)}, f32[2,256,64]{1,2,0:T(8,128)S(1)}, s32[8]{0:T(128)S(1)}, /*index=5*/s32...) while((s32[]{:T(128)}, f32[2,256]{1,0:T(2,128)S(1)}, ...), condition=%wide.region_8.9_spmd.clone, body=%wide.region_3.8_spmd.clone.sunk | while | flops 278465792 | bytes 17209772 | solution.py:239
  414.0 6.1 %conditional.3 = ((f32[2,256]{1,0:T(2,128)S(1)}, f32[2,256]{1,0:T(2,128)S(1)}, f32[2,256,64]{1,2,0:T(8,128)S(1)})) conditional(s32[]{:T(128)} %convert_element_type.113, (f32[2,256]{1,0:T(2,128)S(1)}, f32[2,256]{1,0:T(2,128)S(1)}, f32[2,256,64]{1,2,0:T(8,128)S(1)}) %tuple.39, (s32[]{:T(128)}, s32[]{:T(128)}, s32[]{:T(128)}, ...), branch_computations={%region_4.4_spmd, %region_5.7_spmd} | conditional | flops 278465792 | bytes 17208448 | solution.py:237
  417.2 1.4 fusion.47
  421.3 6.1 %conditional.3 = ((f32[2,256]{1,0:T(2,128)S(1)}, f32[2,256]{1,0:T(2,128)S(1)}, f32[2,256,64]{1,2,0:T(8,128)S(1)})) conditional(s32[]{:T(128)} %convert_element_type.113, (f32[2,256]{1,0:T(2,128)S(1)}, f32[2,256]{1,0:T(2,128)S(1)}, f32[2,256,64]{1,2,0:T(8,128)S(1)}) %tuple.39, (s32[]{:T(128)}, s32[]{:T(128)}, s32[]{:T(128)}, ...), branch_computations={%region_4.4_spmd, %region_5.7_spmd} | conditional | flops 278465792 | bytes 17208448 | solution.py:237
  424.6 1.4 fusion.47
  428.7 6.0 %conditional.3 = ((f32[2,256]{1,0:T(2,128)S(1)}, f32[2,256]{1,0:T(2,128)S(1)}, f32[2,256,64]{1,2,0:T(8,128)S(1)})) conditional(s32[]{:T(128)} %convert_element_type.113, (f32[2,256]{1,0:T(2,128)S(1)}, f32[2,256]{1,0:T(2,128)S(1)}, f32[2,256,64]{1,2,0:T(8,128)S(1)}) %tuple.39, (s32[]{:T(128)}, s32[]{:T(128)}, s32[]{:T(128)}, ...), branch_computations={%region_4.4_spmd, %region_5.7_spmd} | conditional | flops 278465792 | bytes 17208448 | solution.py:237
  436.0 6.1 %conditional.3 = ((f32[2,256]{1,0:T(2,128)S(1)}, f32[2,256]{1,0:T(2,128)S(1)}, f32[2,256,64]{1,2,0:T(8,128)S(1)})) conditional(s32[]{:T(128)} %convert_element_type.113, (f32[2,256]{1,0:T(2,128)S(1)}, f32[2,256]{1,0:T(2,128)S(1)}, f32[2,256,64]{1,2,0:T(8,128)S(1)}) %tuple.39, (s32[]{:T(128)}, s32[]{:T(128)}, s32[]{:T(128)}, ...), branch_computations={%region_4.4_spmd, %region_5.7_spmd} | conditional | flops 278465792 | bytes 17208448 | solution.py:237
  439.2 1.4 fusion.47
  443.3 6.0 %conditional.3 = ((f32[2,256]{1,0:T(2,128)S(1)}, f32[2,256]{1,0:T(2,128)S(1)}, f32[2,256,64]{1,2,0:T(8,128)S(1)})) conditional(s32[]{:T(128)} %convert_element_type.113, (f32[2,256]{1,0:T(2,128)S(1)}, f32[2,256]{1,0:T(2,128)S(1)}, f32[2,256,64]{1,2,0:T(8,128)S(1)}) %tuple.39, (s32[]{:T(128)}, s32[]{:T(128)}, s32[]{:T(128)}, ...), branch_computations={%region_4.4_spmd, %region_5.7_spmd} | conditional | flops 278465792 | bytes 17208448 | solution.py:237
  450.7 6.1 %conditional.3 = ((f32[2,256]{1,0:T(2,128)S(1)}, f32[2,256]{1,0:T(2,128)S(1)}, f32[2,256,64]{1,2,0:T(8,128)S(1)})) conditional(s32[]{:T(128)} %convert_element_type.113, (f32[2,256]{1,0:T(2,128)S(1)}, f32[2,256]{1,0:T(2,128)S(1)}, f32[2,256,64]{1,2,0:T(8,128)S(1)}) %tuple.39, (s32[]{:T(128)}, s32[]{:T(128)}, s32[]{:T(128)}, ...), branch_computations={%region_4.4_spmd, %region_5.7_spmd} | conditional | flops 278465792 | bytes 17208448 | solution.py:237
  458.0 6.0 %conditional.3 = ((f32[2,256]{1,0:T(2,128)S(1)}, f32[2,256]{1,0:T(2,128)S(1)}, f32[2,256,64]{1,2,0:T(8,128)S(1)})) conditional(s32[]{:T(128)} %convert_element_type.113, (f32[2,256]{1,0:T(2,128)S(1)}, f32[2,256]{1,0:T(2,128)S(1)}, f32[2,256,64]{1,2,0:T(8,128)S(1)}) %tuple.39, (s32[]{:T(128)}, s32[]{:T(128)}, s32[]{:T(128)}, ...), branch_computations={%region_4.4_spmd, %region_5.7_spmd} | conditional | flops 278465792 | bytes 17208448 | solution.py:237
  465.3 6.0 %conditional.3 = ((f32[2,256]{1,0:T(2,128)S(1)}, f32[2,256]{1,0:T(2,128)S(1)}, f32[2,256,64]{1,2,0:T(8,128)S(1)})) conditional(s32[]{:T(128)} %convert_element_type.113, (f32[2,256]{1,0:T(2,128)S(1)}, f32[2,256]{1,0:T(2,128)S(1)}, f32[2,256,64]{1,2,0:T(8,128)S(1)}) %tuple.39, (s32[]{:T(128)}, s32[]{:T(128)}, s32[]{:T(128)}, ...), branch_computations={%region_4.4_spmd, %region_5.7_spmd} | conditional | flops 278465792 | bytes 17208448 | solution.py:237
  471.9 19.4 %all_to_all.10 = bf16[4,64,2048]{2,1,0:T(8,128)(2,1)S(1)} all-to-all(bf16[4,64,2048]{2,1,0:T(8,128)(2,1)S(1)} %bitcast.68), channel_id=1, replica_groups=mesh['grp'=2,'sp_0'=32,'sp_1'=2,'tp'=4] {'tp'}, dimensions={0} | all-to-all | bytes 2097152 | tf_op jit(solution)/shard_map/all_to_all | solution.py:71
  (160 shorter events, 58.8 us)
Async XLA Ops:
  6.5 8.3 %copy-start.3 = (bf16[128,32]{0,1:T(8,128)(2,1)S(1)}, bf16[128,32]{0,1:T(8,128)(2,1)}, u32[]{:S(2)}) copy-start(bf16[128,32]{0,1:T(8,128)(2,1)} %param.31) | copy-start | bytes 24580
  6.5 8.3 %copy-start.4 = (bf16[128,32]{0,1:T(8,128)(2,1)S(1)}, bf16[128,32]{0,1:T(8,128)(2,1)}, u32[]{:S(2)}) copy-start(bf16[128,32]{0,1:T(8,128)(2,1)} %param.30) | copy-start | bytes 24580
  6.6 23.8 %copy-start.2 = (f32[2048]{0:T(1024)S(1)}, f32[2048]{0:T(1024)}, u32[]{:S(2)}) copy-start(f32[2048]{0:T(1024)} %param.19) | copy-start | bytes 24580
  6.6 122.5 %all-gather.6.cloned.1.call-start = ((), (), s32[]{:S(2)}) async-start(), calls=%async_computation.2 | async-start | bytes 2662400 | tf_op jit(solution)/shard_map/all_gather | solution.py:35
  10.3 19.7 %all-to-all-start = ((bf16[4,256,512]{1,2,0:T(8,128)(2,1)}), bf16[4,256,512]{1,2,0:T(8,128)(2,1)S(1)}, u32[]{:S(2)}, u32[]{:S(2)}) async-start(bf16[4,256,512]{1,2,0:T(8,128)(2,1)} %broadcast_in_dim.40), calls=%async_computation | async-start | bytes 2097152 | tf_op jit(solution)/shard_map/all_to_all | solution.py:23
  14.8 242.0 %all-gather.8.cloned.1.call-start = ((), (), s32[]{:S(2)}) async-start(), calls=%async_computation.3 | async-start | bytes 1064960 | tf_op jit(solution)/shard_map/all_gather | solution.py:56
  15.6 391.3 %all-gather.10.cloned.1.call-start = ((), (), s32[]{:S(2)}) async-start(), calls=%async_computation.4 | async-start | bytes 8519680 | tf_op jit(solution)/shard_map/all_gather | solution.py:35
  30.3 102.3 %copy-start.6 = (f32[128]{0:T(128)S(1)}, f32[128]{0:T(128)}, u32[]{:S(2)}) copy-start(f32[128]{0:T(128)} %param.28) | copy-start | bytes 1540
  30.3 102.4 %copy-start.5 = (f32[2]{0:T(128)S(1)}, f32[2]{0:T(128)}, u32[]{:S(2)}) copy-start(f32[2]{0:T(128)} %param.26) | copy-start | bytes 28
  194.7 2.1 copy-start.1
  412.7 58.7 %copy-start = (bf16[2048,256]{1,0:T(8,128)(2,1)S(1)}, bf16[2048,256]{1,0:T(8,128)(2,1)}, u32[]{:S(2)}) copy-start(bf16[2048,256]{1,0:T(8,128)(2,1)} %all-gather.8.cloned.1.call-done) | copy-start | bytes 3145732
Sparse Core Ops, SparseCore 0:
  9.5 119.5 all-gather.5
  131.2 125.6 all-gather.7
  258.9 147.8 all-gather.9
where the time goes:
time: 501 us; the launch traced here: 499 us
  waiting for transfers between devices  319 us (64%)
  blocking collectives  77.1 us (15%)
  local copies, waits for them, and re-layouts  31.8 us (6%)
  matrix products  29.6 us (6%)
  between operations  13.3 us (3%)
  other arithmetic  11.7 us (2%)
  loops' own time  11.4 us (2%)
    all_gather x2, waiting for transfers between devices, sent_together(): result = lax.all_gather(both, axis, axis=dim, tiled=True)  247 us
    all_gather x1, waiting for transfers between devices, rows_first(): lax.all_gather(both, axis, axis=0, tiled=True)  57.8 us
    all_gather x2, blocking collectives, all_blocks(): blocks = lax.all_gather(blocks, axes[k])  57.6 us
    all_to_all x1, blocking collectives, summed_on_arrival(): lax.all_to_all(blocks, axis, split_axis=0, concat_axis=0, tiled=True)  19.4 us
    all_to_all x1, waiting for transfers between devices, from_everyone(): lax.all_to_all(jnp.broadcast_to(array[None], (count, *array.shape)), axis...  14.3 us
    dot_general x8, matrix products, softmax_update(): jnp.einsum('qhd,khd->hqk', query_heads, key_block, preferred_element_type...  11.2 us
    dynamic_slice x8, local copies, waits for them, and re-layouts, compute(): lax.dynamic_slice_in_dim(value_rows, number * block_rows, block_rows, 0)  10.2 us
  transfers between devices with their start and end apart: 4, of which 4 were waited for; matrix products, arithmetic and copies ran while one was open for 3% of the time, Pallas kernels for 0%

commit v1 on v0

v1 whole, which is shorter than its diff:
```python
import functools
import math

import jax
import jax.numpy as jnp
from jax import lax
from jax.experimental import pallas as pl
from jax.experimental.pallas import tpu as pltpu
from jax.sharding import PartitionSpec as P

MESH = pl.DeviceIdType.MESH
EPS = 1e-06
F32 = jnp.float32
BF16 = jnp.bfloat16
LOG2E = 1.4426950408889634
LOW = -3.0e38


def nt(a, b):
    return lax.dot_general(a, b, (((1,), (1,)), ((), ())), preferred_element_type=F32)


def nn(a, b):
    return jnp.dot(a, b, preferred_element_type=F32)


def split(a):
    high = a.astype(BF16)
    return high, (a - high.astype(F32)).astype(BF16)


def kernel(
    Z, X,
    tok, gain, rqw, rkw, rvw, fqw, fkw, fvw, dec, state, hng, gates, row, fow,
    out,
    wall, wsend, tokall, normed, kv, qbuf, rbuf, rin, summ, dall, mx, tot, acc, ot, mix, mixall,
    swap_s, swap_r, tok_s, tok_r, tokc_s, tokc_r, tok_l, ws, wr, ks, kr, ss, sr,
    ot_s, ot_r, otc_s, otc_r, ot_l, mix_s, mix_r,
):
    sp = lax.axis_index("sp")
    x = lax.axis_index("tp")
    c = lax.rem(sp, 2)
    z = sp // 2
    H = Z // 2
    rows_w = rqw.shape[0]
    chip_w = 2 * rows_w
    D = gain.shape[1]
    T, feat = tok.shape
    C = 2 * T
    Q = C // 4
    out_rows = T // X

    def at_z(k):
        return {"sp": lax.rem(z + k + Z, Z) * 2 + c}

    right, left = at_z(1), at_z(-1)
    sib = {"sp": z * 2 + 1 - c}
    peers = [{"tp": lax.rem(x + r, X)} for r in range(1, X)]
    cross = [{"tp": lax.rem(x + r, X), "sp": z * 2 + 1 - c} for r in range(1, X)]

    def remote(src, dst, s, r, dev):
        return pltpu.make_async_remote_copy(
            src_ref=src, dst_ref=dst, send_sem=s, recv_sem=r, device_id=dev, device_id_type=MESH
        )

    def head_block(h):
        def cut(ref, width):
            return ref[:, h * width : (h + 1) * width].astype(F32)

        half = rqw.shape[1] // 2
        wide = rvw.shape[1] // 2
        kvw = jnp.concatenate([cut(fkw, wide), cut(fvw, wide)], axis=1)
        rw = jnp.concatenate([cut(rvw, wide), cut(rqw, half), cut(rkw, half)], axis=1)
        fq = cut(fqw, wide)
        qw = jnp.concatenate([fq, jnp.zeros_like(fq)], axis=1)
        return kvw, rw, qw

    first, second = head_block(0), head_block(1)
    outs = jnp.concatenate(
        [row[...].astype(F32), fow[...].astype(F32), jnp.zeros((row.shape[0], 64), F32)], axis=1
    ).T
    ro, fo = outs[:rows_w], outs[rows_w : 2 * rows_w]
    wide = ro.shape[1] // 2
    out_first = jnp.concatenate([ro[:, :wide], fo[:, :wide]], axis=1)
    out_second = jnp.concatenate([ro[:, wide:], fo[:, wide:]], axis=1)
    is0 = c == 0
    own_rows = pl.ds(pl.multiple_of(z * chip_w + c * rows_w, rows_w), rows_w)
    blocks = [(first[0], second[0]), (first[1], second[1]), (out_first, out_second), (first[2], second[2])]
    for k, (a, b) in enumerate(blocks):
        wall[k, own_rows, :] = jnp.where(is0, a, b).astype(BF16)
        wsend[k] = jnp.where(is0, b, a).astype(BF16)

    barrier = pltpu.get_barrier_semaphore()
    partners = [right, left, sib] + peers + cross
    for dev in partners:
        pl.semaphore_signal(barrier, inc=1, device_id=dev, device_id_type=MESH)
    pl.semaphore_wait(barrier, len(partners))

    swap = remote(wsend, wall.at[:, own_rows, :], swap_s, swap_r, sib)
    swap.start()

    def tok_at(core, member):
        return tokall.at[core, :, pl.ds(pl.multiple_of(member * feat, feat), feat)]

    def source(r):
        return lax.rem(x - r + X, X)

    tok_sends = [remote(tok, tok_at(c, x), tok_s.at[r], tok_r.at[r], peers[r]) for r in range(X - 1)]
    for copy in tok_sends:
        copy.start()
    tok_cross = [remote(tok, tok_at(c, x), tokc_s.at[0], tokc_r.at[0], sib)]
    for r in range(1, X):
        tok_cross.append(
            remote(tok_at(c, source(r)), tok_at(c, source(r)), tokc_s.at[r], tokc_r.at[r], sib)
        )
    tok_cross[0].start()
    tok_own = pltpu.make_async_copy(tok, tok_at(c, x), tok_l)
    tok_own.start()

    gate_ref = jnp.where(is0, gates[0:1, pl.ds(pl.multiple_of(z * C, C), 128)], gates[1:2, pl.ds(pl.multiple_of(z * C, C), 128)])
    gate_row = jnp.where(is0, gates[0:1, :], gates[1:2, :])
    dall[...] = (gate_ref[:, 0:1] - gate_row) * LOG2E

    swap.wait()

    def ring_copy(buf_at, way, k, o, sems_s, sems_r, s):
        where = buf_at(k, o)
        return remote(where, where, sems_s.at[way, k], sems_r.at[way, s - 1, k], right if way == 0 else left)

    def origin(way, s):
        return lax.rem(z - s + Z, Z) if way == 0 else lax.rem(z + s, Z)

    def ring_start(buf_at, sems_s, sems_r, k):
        for way in range(2):
            ring_copy(buf_at, way, k, z, sems_s, sems_r, 1).start()

    def ring_step(buf_at, sems_s, sems_r, s, k):
        def one(way, mine):
            @pl.when(jnp.logical_or(s < H, mine))
            def _():
                o = origin(way, s)
                ring_copy(buf_at, way, k, o, sems_s, sems_r, s).wait_recv()

                @pl.when(jnp.logical_or(s + 1 < H, jnp.logical_and(s < H, mine)))
                def _():
                    nxt = ring_copy(buf_at, way, k, o, sems_s, sems_r, s + 1)
                    nxt.wait_send()
                    nxt.start()

        one(0, k < 2)
        one(1, k >= 2)

    def ring_end(buf_at, sems_s, sems_r, k):
        for way in range(2):
            ring_copy(buf_at, way, k, z, sems_s, sems_r, 1).wait_send()

    def wall_at(k, o):
        return wall.at[k, pl.ds(pl.multiple_of(o * chip_w, chip_w), chip_w), :]

    for k in range(4):
        ring_start(wall_at, ws, wr, k)

    pieces = 8
    stride = max(1, 4 * H // (2 * pieces))
    base = 4 * H - pieces * stride
    tok_step = base * 3 // 4
    P_rows = C // pieces

    def normalize(p):
        at = lax.rem(c * (pieces // 2) + p, pieces)
        half = at // (pieces // 2)
        lines = pl.ds(pl.multiple_of(lax.rem(at, pieces // 2) * P_rows, P_rows), P_rows)
        wide_rows = tokall[half, lines, :].astype(F32)
        scale = lax.rsqrt(jnp.mean(wide_rows * wide_rows, axis=1, keepdims=True) + EPS)
        normed[pl.ds(pl.multiple_of(at * P_rows, P_rows), P_rows), :] = (
            wide_rows * scale * gain[...]
        ).astype(BF16)

    def weights_loop(idx, carry):
        s = idx // 4 + 1
        k = lax.rem(idx, 4)
        ring_step(wall_at, ws, wr, s, k)

        @pl.when(idx == tok_step)
        def _():
            tok_own.wait()
            for r in range(1, X):
                tok_sends[r - 1].wait_recv()
                tok_cross[r].start()

        @pl.when(jnp.logical_and(idx >= base, lax.rem(idx - base, stride) == 0))
        def _():
            p = (idx - base) // stride

            @pl.when(p == pieces // 2)
            def _():
                for copy in tok_cross:
                    copy.wait_recv()

            normalize(p)

        return carry

    lax.fori_loop(0, 4 * H, weights_loop, 0)

    def project(k, dst, first_row):
        def body(i, carry):
            rows = pl.ds(pl.multiple_of(i * Q, Q), Q)
            dst[pl.ds(pl.multiple_of(first_row + i * Q, Q), Q), :] = nn(normed[rows, :], wall[k]).astype(BF16)
            return carry

        lax.fori_loop(0, 4, body, 0)

    def kv_at(k, o):
        return kv.at[pl.ds(pl.multiple_of(o * C + k * Q, Q), Q), :]

    def summ_at(k, o):
        return summ.at[o]

    project(0, kv, z * C)
    for k in range(3):
        ring_start(kv_at, ks, kr, k)
    project(3, qbuf, 0)
    ring_start(kv_at, ks, kr, 3)
    project(1, rbuf, 0)

    def ot_at(member, core):
        return ot.at[member, :, pl.ds(pl.multiple_of(core * 128, 128), 128)]

    ot_sends = [remote(wall.at[2], ot_at(x, c), ot_s.at[r], ot_r.at[r], peers[r]) for r in range(X - 1)]
    for copy in ot_sends:
        copy.start()
    ot_cross = [remote(wall.at[2], ot_at(x, c), otc_s.at[0], otc_r.at[0], sib)]
    for r in range(1, X):
        ot_cross.append(
            remote(ot_at(source(r), c), ot_at(source(r), c), otc_s.at[r], otc_r.at[r], sib)
        )
    ot_cross[0].start()
    ot_own = pltpu.make_async_copy(wall.at[2], ot_at(x, c), ot_l)
    ot_own.start()

    a = jnp.where(is0, dec[0], dec[1])
    key_size = rqw.shape[1] // 2
    key_scale = key_size ** (-0.5)
    lane = lax.broadcasted_iota(jnp.int32, (C, 128), 1)
    sub = lax.broadcasted_iota(jnp.int32, (C, 128), 0)
    trail = jnp.exp((C - 1.0 - sub.astype(F32)) * a) * key_scale
    turned = (rbuf[...].astype(F32) * trail).T
    t_high, t_low = split(turned)
    grown = nn(t_high, rbuf[...]) + nn(t_low, rbuf[...])
    lane16 = lax.broadcasted_iota(jnp.int32, (16, 128), 1)
    summ[z] = jnp.where(lane16 < 64, grown[96:112, :], pltpu.roll(grown[112:128, :], 64, 1))

    mx[...] = jnp.full_like(mx, LOW)
    tot[...] = jnp.zeros_like(tot)
    acc[...] = jnp.zeros_like(acc)
    fox_scale = (fqw.shape[1] // 2) ** (-0.5) * LOG2E

    def attend(i, j, masked):
        rows = pl.ds(pl.multiple_of(i * Q, Q), Q)
        block = kv[pl.ds(pl.multiple_of(j * C, C), C), :]
        s = nt(qbuf[rows, :], block) * fox_scale + dall[:, pl.ds(pl.multiple_of(j * C, C), C)]
        if masked:
            q_at = lax.broadcasted_iota(jnp.int32, s.shape, 0) + i * Q
            k_at = lax.broadcasted_iota(jnp.int32, s.shape, 1)
            s = jnp.where(k_at <= q_at, s, LOW)
        old = mx[rows, :]
        new = jnp.maximum(old, jnp.max(s, axis=1, keepdims=True))
        alpha = jnp.exp2(old - new)
        parts = [jnp.exp2(s[:, n * 128 : (n + 1) * 128] - new) for n in range(C // 128)]
        total = alpha * tot[rows, :]
        for part in parts:
            total = total + part
        tot[rows, :] = total
        mx[rows, :] = new
        weights = jnp.concatenate([part.astype(BF16) for part in parts], axis=1)
        acc[rows, :] = alpha * acc[rows, :] + nn(weights, block)

    def inner(i):
        rows = pl.ds(pl.multiple_of(i * Q, Q), Q)
        lanes = lax.broadcasted_iota(jnp.int32, (Q, 128), 1)
        query = jnp.where(jnp.logical_and(lanes >= 64, lanes < 96), rbuf[rows, :].astype(F32), 0.0).astype(BF16)
        keys = pltpu.roll(rbuf[...].astype(F32), 96, 1).astype(BF16)
        s = nt(query, keys)
        gap = lax.broadcasted_iota(jnp.int32, s.shape, 0) + i * Q - lax.broadcasted_iota(jnp.int32, s.shape, 1)
        within = jnp.where(gap >= 0, jnp.exp(jnp.maximum(gap, 0).astype(F32) * a), 0.0)
        high, low = split(s * key_scale * within)
        rin[rows, :] = nn(high, rbuf[...]) + nn(low, rbuf[...])

    def past(i, s):
        @pl.when(z - s >= 0)
        def _():
            attend(i, z - s, False)

        @pl.when(jnp.logical_and(z + s >= Z, s < H))
        def _():
            attend(i, z + s - Z, False)

    def attend_loop(idx, carry):
        s = idx // 4 + 1
        k = lax.rem(idx, 4)
        ring_step(kv_at, ks, kr, s, k)

        @pl.when(k == 3)
        def _():
            for way in range(2):
                @pl.when(jnp.logical_or(s < H, way == 0))
                def _(way=way):
                    o = origin(way, s)
                    ring_copy(summ_at, way, 0, o, ss, sr, s).wait_recv()

                    @pl.when(jnp.logical_or(s + 1 < H, jnp.logical_and(s < H, way == 0)))
                    def _():
                        nxt = ring_copy(summ_at, way, 0, o, ss, sr, s + 1)
                        nxt.wait_send()
                        nxt.start()

        @pl.when(s == 1)
        def _():
            inner(k)
            attend(k, z, True)

        @pl.when(s > 1)
        def _():
            past(k, s - 1)

        @pl.when(idx == 4 * H - 8)
        def _():
            for r in range(1, X):
                ot_sends[r - 1].wait_recv()
                ot_cross[r].start()

        return carry

    ring_start(summ_at, ss, sr, 0)
    lax.fori_loop(0, 4 * H, attend_loop, 0)

    def last(i, carry):
        past(i, H)
        return carry

    lax.fori_loop(0, 4, last, 0)

    span = float(C)
    far = z.astype(F32) * span

    def gather_state(j, total):
        gap = jnp.maximum(z - 1 - j, 0).astype(F32) * span
        weight = jnp.where(j < z, jnp.exp(jnp.zeros((16, 128), F32) + gap * a), 0.0)
        return total + weight * summ[j]

    packed = lax.fori_loop(0, Z, gather_state, jnp.zeros((16, 128), F32))
    both = jnp.concatenate([packed, pltpu.roll(packed, 64, 1)], axis=0)
    start = jnp.where(is0, state[0], state[1])
    start = jnp.concatenate([start, jnp.zeros_like(start)], axis=1)
    lane32 = lax.broadcasted_iota(jnp.int32, (32, 128), 1)
    entering = jnp.where(lane32 < 64, both, 0.0) + jnp.exp(jnp.zeros((32, 128), F32) + far * a) * start
    entering = jnp.concatenate([jnp.zeros((64, 128), F32), entering, jnp.zeros((32, 128), F32)], axis=0)
    e_high, e_low = split(entering)
    hn = hng[...]
    hn = jnp.where(is0, hn, pltpu.roll(hn, 64, 1))

    def finish(i, carry):
        rows = pl.ds(pl.multiple_of(i * Q, Q), Q)
        lanes = lax.broadcasted_iota(jnp.int32, (Q, 128), 1)
        place = (lax.broadcasted_iota(jnp.int32, (Q, 128), 0) + i * Q).astype(F32)
        leading = jnp.exp((place + 1.0) * a)
        query = rbuf[rows, :]
        raw = rin[rows, :] + (nn(query, e_high) + nn(query, e_low)) * leading
        raw = jnp.where(lanes < 64, raw, 0.0)
        center = jnp.where(lanes < 64, raw - jnp.sum(raw, axis=1, keepdims=True) * (1.0 / 64), 0.0)
        spread = jnp.sum(center * center, axis=1, keepdims=True) * (1.0 / 64)
        ret = center * lax.rsqrt(spread + EPS) * hn
        fox = acc[rows, :] / jnp.sum(tot[rows, :], axis=1, keepdims=True)
        mix[rows, :] = jnp.where(lanes < 64, ret, fox).astype(BF16)
        return carry

    lax.fori_loop(0, 4, finish, 0)

    def mix_rows(core, member):
        return mix.at[pl.ds(pl.multiple_of(core * T + member * out_rows, out_rows), out_rows), :]

    here = mixall.at[x, :, pl.ds(pl.multiple_of(c * 128, 128), 128)]
    mix_sends = [remote(mix_rows(1 - c, x), here, mix_s.at[0], mix_r.at[0], sib)]
    for r in range(1, X):
        member = lax.rem(x + r, X)
        mix_sends.append(remote(mix_rows(c, member), here, mix_s.at[2 * r - 1], mix_r.at[2 * r - 1], peers[r - 1]))
        mix_sends.append(remote(mix_rows(1 - c, member), here, mix_s.at[2 * r], mix_r.at[2 * r], cross[r - 1]))
    for copy in mix_sends:
        copy.start()
    mixall[x, :, pl.ds(pl.multiple_of(c * 128, 128), 128)] = mix[
        pl.ds(pl.multiple_of(c * T + x * out_rows, out_rows), out_rows), :
    ]
    ot_own.wait()
    for copy in ot_cross:
        copy.wait_recv()
    for copy in mix_sends:
        copy.wait_recv()

    tile = 256

    def project_out(n, carry):
        cols = pl.ds(pl.multiple_of(n * tile, tile), tile)
        total = jnp.zeros((out_rows, tile), F32)
        for g in range(X):
            total = total + nt(mixall[g], ot[g, cols, :]).astype(BF16).astype(F32)
        out[:, cols] = total.astype(BF16)
        return carry

    lax.fori_loop(0, D // tile, project_out, 0)

    for copy in tok_sends + tok_cross + ot_sends + ot_cross + mix_sends:
        copy.wait_send()
    for k in range(4):
        ring_end(wall_at, ws, wr, k)
        ring_end(kv_at, ks, kr, k)
    ring_end(summ_at, ss, sr, 0)


def local(Z, X, tokens, norm_gain, rqw, rkw, rvw, fqw, fkw, fvw, decay, state, hng, gates, row, fow):
    T = tokens.shape[0]
    C = 2 * T
    D = norm_gain.shape[0]
    H = Z // 2
    vm = pl.BlockSpec(memory_space=pltpu.VMEM)
    dma = pltpu.SemaphoreType.DMA
    in_specs = [vm] * 14
    in_specs[8] = pl.BlockSpec(memory_space=pltpu.SMEM)
    return pl.pallas_call(
        functools.partial(kernel, Z, X),
        out_shape=jax.ShapeDtypeStruct((T // X, D), BF16),
        in_specs=in_specs,
        out_specs=vm,
        scratch_shapes=[
            pltpu.VMEM((4, D, 128), BF16),
            pltpu.VMEM((4, rqw.shape[0], 128), BF16),
            pltpu.VMEM((2, T, D), BF16),
            pltpu.VMEM((C, D), BF16),
            pltpu.VMEM((Z * C, 128), BF16),
            pltpu.VMEM((C, 128), BF16),
            pltpu.VMEM((C, 128), BF16),
            pltpu.VMEM((C, 128), F32),
            pltpu.VMEM((Z, 16, 128), F32),
            pltpu.VMEM((1, Z * C), F32),
            pltpu.VMEM((C, 128), F32),
            pltpu.VMEM((C, 128), F32),
            pltpu.VMEM((C, 128), F32),
            pltpu.VMEM((X, D, 256), BF16),
            pltpu.VMEM((C, 128), BF16),
            pltpu.VMEM((X, T // X, 256), BF16),
            dma, dma,
            dma((X - 1,)), dma((X - 1,)), dma((X,)), dma((X,)), dma,
            dma((2, 4)), dma((2, H, 4)),
            dma((2, 4)), dma((2, H, 4)),
            dma((2, 1)), dma((2, H, 1)),
            dma((X - 1,)), dma((X - 1,)), dma((X,)), dma((X,)), dma,
            dma((2 * X - 1,)), dma((2 * X - 1,)),
        ],
        compiler_params=pltpu.CompilerParams(
            collective_id=0, has_side_effects=True, vmem_limit_bytes=56 * 1024 * 1024
        ),
    )(
        tokens, norm_gain.reshape(1, -1), rqw, rkw, rvw, fqw, fkw, fvw, decay, state,
        hng.reshape(1, -1), gates.T, row, fow,
    )


def solution(mesh):
    Z, X = mesh.shape["sp"] // 2, mesh.shape["tp"]
    return jax.shard_map(
        functools.partial(local, Z, X),
        mesh=mesh,
        in_specs=(
            P(("grp", "sp"), "tp"),
            P(),
            P("sp", "tp"),
            P("sp", "tp"),
            P("sp", "tp"),
            P("sp", "tp"),
            P("sp", "tp"),
            P("sp", "tp"),
            P("tp"),
            P(("grp", "tp"), None, None),
            P("tp"),
            P("grp", "tp"),
            P("tp", "sp"),
            P("tp", "sp"),
        ),
        out_specs=P(("grp", "sp", "tp"), None),
        check_vma=False,
    )
```

time: 501 us -> 181 us (0.36)
  the two profiles are of different devices: /device:TPU:1888 before, /device:TPU:33 now
where the time goes in v1:
time: 181 us
  Pallas kernels  177 us (98%)
  local copies, waits for them, and re-layouts  3.81 us (2%)
    pallas_call x1, Pallas kernels, local(): pl.pallas_call(functools.partial(kernel, Z, X), out_shape=jax.ShapeDtypeS...  177 us
    unnamed x5, local copies, waits for them, and re-layouts  3.81 us

profile of v1, /device:TPU:33, one launch (start us, length us, event | category | flops | bytes accessed | tf_op | source)
XLA Modules:
  0.0 180.9 jit_solution(12586359863838255310)
XLA Ops:
  0.0 0.0 copy-start
  0.0 1.4 copy.15.row
  1.4 0.0 copy-done
  1.4 0.7 copy.16.fow
  2.1 177.1 %shard_map.136 = bf16[64,2048]{1,0:T(8,128)(2,1)} custom-call(bf16[256,512]{1,0:T(8,128)(2,1)} %tok.1, f32[1,2048]{1,0:T(1,128)} %bitcast.4, bf16[32,64]{1,0:T(8,128)(2,1)} %rqw.1, bf16[32,64]{1,0:T(8,128)(2,1)} %rkw.1, bf16[32,128]{1,0:T(8,128)(2,1)} %rvw.1, bf16[32,128]{1,0:T(8,128)(2,1)} %fqw.1, bf16[32,128]{1,0:T(8,128)(2,1)} %fkw.1, ...), custom_call_target="tpu_custom_call" | custom-call | tf_op jit(solution)/shard_map/pallas_call | solution.py:429
  179.2 1.7 copy.18
Async XLA Ops:
  0.0 1.4 copy-start

commit v2 on v1

v2 whole, which is shorter than its diff:
```python
import functools
import math

import jax
import jax.numpy as jnp
from jax import lax
from jax.experimental import pallas as pl
from jax.experimental.pallas import tpu as pltpu
from jax.sharding import PartitionSpec as P

MESH = pl.DeviceIdType.MESH
EPS = 1e-06
F32 = jnp.float32
BF16 = jnp.bfloat16
LOG2E = 1.4426950408889634
LOW = -3.0e38


def nt(a, b):
    return lax.dot_general(a, b, (((1,), (1,)), ((), ())), preferred_element_type=F32)


def nn(a, b):
    return jnp.dot(a, b, preferred_element_type=F32)


def split(a):
    high = a.astype(BF16)
    return high, (a - high.astype(F32)).astype(BF16)


def kernel(
    Z, X,
    tok, gain, rqw, rkw, rvw, fqw, fkw, fvw, dec, state, hng, gates, row, fow,
    out,
    wide_w, out_w, pack_w, query_w, send_w, send_o, send_p,
    tokall, normed, kv, qbuf, rbuf, rin, summ, dall, mx, tot, acc, ot, mix, mixall,
    swap_s, swap_r, tok_s, tok_r, tokc_s, tokc_r, tok_l, ws, wr, ks, kr, kl, ready,
    ot_s, ot_r, otc_s, otc_r, ot_l, mix_s, mix_r,
):
    sp = lax.axis_index("sp")
    x = lax.axis_index("tp")
    c = lax.rem(sp, 2)
    z = sp // 2
    H = Z // 2
    rows_w = rqw.shape[0]
    chip_w = 2 * rows_w
    D = gain.shape[1]
    T, feat = tok.shape
    C = 2 * T
    Q = C // 4
    out_rows = T // X
    is0 = c == 0

    def at_z(k):
        return {"sp": lax.rem(z + k + Z, Z) * 2 + c}

    hops = [(at_z(1), at_z(2)), (at_z(-1), at_z(-2))]
    sib = {"sp": z * 2 + 1 - c}
    final = {"sp": (Z - 1) * 2 + c}
    peers = [{"tp": lax.rem(x + r, X)} for r in range(1, X)]
    cross = [{"tp": lax.rem(x + r, X), "sp": z * 2 + 1 - c} for r in range(1, X)]

    def remote(src, dst, s, r, dev):
        return pltpu.make_async_remote_copy(
            src_ref=src, dst_ref=dst, send_sem=s, recv_sem=r, device_id=dev, device_id_type=MESH
        )

    def block(n, size):
        return pl.ds(pl.multiple_of(n * size, size), size)

    def head_block(h):
        def cut(ref):
            width = ref.shape[1] // 2
            return ref[:, h * width : (h + 1) * width].astype(F32)

        fq = cut(fqw)
        half = fq.shape[0] // 2
        return (
            jnp.concatenate([cut(fkw), cut(fvw), cut(rvw), cut(rqw), cut(rkw)], axis=1),
            jnp.concatenate([cut(row), cut(fow)], axis=1),
            jnp.concatenate([fq[:half], fq[half:]], axis=1),
        )

    first, second = head_block(0), head_block(1)
    own_rows = block(2 * z + c, rows_w)
    own_pack = block(2 * z + c, rows_w // 2)
    wide_w[own_rows, :] = jnp.where(is0, first[0], second[0]).astype(BF16)
    out_w[own_rows, :] = jnp.where(is0, first[1], second[1]).astype(BF16)
    pack_w[own_pack, :] = jnp.where(is0, first[2], second[2]).astype(BF16)
    send_w[...] = jnp.where(is0, second[0], first[0]).astype(BF16)
    send_o[...] = jnp.where(is0, second[1], first[1]).astype(BF16)
    send_p[...] = jnp.where(is0, second[2], first[2]).astype(BF16)

    barrier = pltpu.get_barrier_semaphore()
    partners = [hops[0][0], hops[0][1], hops[1][0], hops[1][1], sib] + peers + cross
    for dev in partners:
        pl.semaphore_signal(barrier, inc=1, device_id=dev, device_id_type=MESH)
    early = z <= H - 2
    is_last = z == Z - 1

    @pl.when(early)
    def _():
        pl.semaphore_signal(barrier, inc=1, device_id=final, device_id_type=MESH)

    pl.semaphore_wait(barrier, len(partners) + jnp.where(is_last, H - 1, 0))

    @pl.when(is_last)
    def _():
        for j in range(H - 1):
            pl.semaphore_signal(ready, inc=1, device_id={"sp": 2 * j + c}, device_id_type=MESH)

    swaps = [
        remote(send_w, wide_w.at[own_rows, :], swap_s.at[0], swap_r.at[0], sib),
        remote(send_o, out_w.at[own_rows, :], swap_s.at[1], swap_r.at[1], sib),
        remote(send_p, pack_w.at[own_pack, :], swap_s.at[2], swap_r.at[2], sib),
    ]
    for copy in swaps:
        copy.start()

    def source(r):
        return lax.rem(x - r + X, X)

    near = sorted({1, X - 1})

    def row_gather(src, at, s, r, cs, cr, local_sem):
        sends = [remote(src, at(x), s.at[n - 1], r.at[n - 1], peers[n - 1]) for n in near]
        over = [remote(src, at(x), cs.at[0], cr.at[0], sib)]
        over += [remote(at(source(n)), at(source(n)), cs.at[n], cr.at[n], sib) for n in near]
        own = pltpu.make_async_copy(src, at(x), local_sem)
        relays, later = [], []
        if X > 2:
            member = jnp.where(is0, source(1), source(X - 1))
            to = jnp.where(is0, lax.rem(x + 1, X), lax.rem(x + X - 1, X))
            relays = [remote(at(member), at(member), s.at[1], r.at[1], {"tp": to})]
            later = [remote(at(source(2)), at(source(2)), cs.at[2], cr.at[2], sib)]

        def begin():
            for copy in sends + over[:1]:
                copy.start()
            own.start()

        def middle():
            for copy in sends:
                copy.wait_recv()
            for copy in relays + over[1:]:
                copy.start()

        def close():
            own.wait()
            for copy in relays:
                copy.wait_recv()
            for copy in later:
                copy.start()

        def arrived():
            for copy in over + later:
                copy.wait_recv()

        def sent():
            for copy in sends + over + relays + later:
                copy.wait_send()

        return begin, middle, close, arrived, sent

    tok_all = row_gather(
        tok, lambda member: tokall.at[c, :, block(member, feat)], tok_s, tok_r, tokc_s, tokc_r, tok_l
    )
    tok_all[0]()

    nearby = gates[:, block(z, C)]
    gate_ref = jnp.where(is0, nearby[0:1, 0:128], nearby[1:2, 0:128])
    dall[...] = (gate_ref[:, 0:1] - jnp.where(is0, gates[0:1, :], gates[1:2, :])) * LOG2E

    for copy in swaps:
        copy.wait()

    def w_at(k, o):
        if k < 2:
            return wide_w.at[block(2 * o + k, rows_w), :]
        if k == 2:
            return out_w.at[block(o, chip_w), :]
        return pack_w.at[block(o, rows_w), :]

    def origin(way, d):
        return lax.rem(z - d + Z, Z) if way == 0 else lax.rem(z + d, Z)

    def w_copy(way, k, reach, o, t):
        return remote(
            w_at(k, o), w_at(k, o), ws.at[way, reach, k], wr.at[way, reach, t, k], hops[way][reach]
        )

    last_t = H // 2 - 1

    def w_step(t, k):
        for way in range(2):
            o = origin(way, 2 * t)

            @pl.when(t > 0)
            def _(way=way, o=o):
                w_copy(way, k, 1, o, t - 1).wait_recv()
                w_copy(way, k, 0, o, t).wait_send()

            w_copy(way, k, 0, o, t).start()
            mine = (k < 2) == (way == 0)

            def pass_two(way=way, o=o):
                @pl.when(t > 0)
                def _():
                    w_copy(way, k, 1, o, t).wait_send()

                w_copy(way, k, 1, o, t).start()

            if mine:
                pass_two()
            else:
                pl.when(t < last_t)(pass_two)

    pieces = 8
    P_rows = C // pieces
    rounds = last_t + 1
    w_total = 4 * rounds
    base = w_total // 2 + 1
    stride = 2
    inside = min(pieces, (w_total - base + stride - 1) // stride)

    def normalize(p):
        @pl.when(p == pieces // 2)
        def _():
            tok_all[3]()

        at = lax.rem(c * (pieces // 2) + p, pieces)
        half = at // (pieces // 2)
        values = tokall[half, block(lax.rem(at, pieces // 2), P_rows), :].astype(F32)
        scale = lax.rsqrt(jnp.mean(values * values, axis=1, keepdims=True) + EPS)
        normed[block(at, P_rows), :] = (values * scale * gain[...]).astype(BF16)

    def weights_loop(t, carry):
        for k in range(4):
            w_step(t, k)
            idx = 4 * t + k

            @pl.when(idx == w_total // 4)
            def _():
                tok_all[1]()

            @pl.when(idx == w_total // 2)
            def _():
                tok_all[2]()

            if k % 2 == 1:

                @pl.when(jnp.logical_and(idx >= base, idx < base + stride * inside))
                def _():
                    normalize((idx - base) // stride)

        return carry

    lax.fori_loop(0, rounds, weights_loop, 0)
    for p in range(inside, pieces):
        normalize(jnp.int32(p))

    def weights_end(t, carry):
        for k in range(4):
            for way in range(2):
                w_copy(way, k, 0, origin(way, 2 * t + 1), t).wait_recv()
        return carry

    lax.fori_loop(0, rounds, weights_end, 0)
    for k in range(4):
        way = 0 if k < 2 else 1
        w_copy(way, k, 1, origin(way, H), last_t).wait_recv()

    def project_wide(i, carry):
        rows = block(i, Q)
        both = nn(normed[rows, :], wide_w[...]).astype(BF16)
        kv[block(z * 4 + i, Q), :] = both[:, :128]
        rbuf[rows, :] = both[:, 128:]
        return carry

    lax.fori_loop(0, 4, project_wide, 0)

    def kv_at(k, o):
        return kv.at[block(o * 4 + k, Q), :] if k < 4 else summ.at[o]

    def right_copy(k, o, s):
        return remote(kv_at(k, o), kv_at(k, o), ks.at[0, k], kr.at[s - 1, k], hops[0][0])

    def left_copy(k, j, dev):
        return remote(kv_at(k, j), kv_at(k, j), ks.at[1, k], kl.at[j, k], dev)

    def kv_start(k):
        @pl.when(z < Z - 1)
        def _():
            right_copy(k, z, 1).start()

        @pl.when(early)
        def _():
            left_copy(k, jnp.minimum(z, H - 2), final).start()

    def left_block(s):
        return s - 2 - (Z - 1 - z)

    def kv_step(k, s):
        @pl.when(z - s >= 0)
        def _():
            o = z - s
            right_copy(k, o, s).wait_recv()

            @pl.when(jnp.logical_and(z < Z - 1, s < H))
            def _():
                nxt = right_copy(k, o, s + 1)
                nxt.wait_send()
                nxt.start()

        j = left_block(s)

        @pl.when(j >= 0)
        def _():
            copy = left_copy(k, j, hops[1][0])
            copy.wait_recv()

            @pl.when(j <= z - H - 2)
            def _():
                @pl.when(j >= 1)
                def _():
                    copy.wait_send()

                copy.start()

    def kv_end(k):
        @pl.when(z < Z - 1)
        def _():
            right_copy(k, z, 1).wait_send()

        @pl.when(jnp.logical_or(early, z >= H + 2))
        def _():
            left_copy(k, 0, final).wait_send()

    @pl.when(early)
    def _():
        pl.semaphore_wait(ready, 1)

    for k in range(4):
        kv_start(k)

    ot_all = row_gather(
        out_w, lambda member: ot.at[member, :, block(c, 128)], ot_s, ot_r, otc_s, otc_r, ot_l
    )
    ot_all[0]()

    lane_p = lax.broadcasted_iota(jnp.int32, (rows_w, 128), 1) < 64
    half_w = rows_w // 2

    def unpack(o, carry):
        packed = pack_w[block(o, rows_w), :].astype(F32)
        low = jnp.where(lane_p, packed, 0.0)
        high = jnp.where(lane_p, pltpu.roll(packed, 64, 1), 0.0)
        query_w[block(o, chip_w), :] = jnp.concatenate(
            [low[:half_w], high[:half_w], low[half_w:], high[half_w:]], axis=0
        ).astype(BF16)
        return carry

    lax.fori_loop(0, Z, unpack, 0, unroll=4)

    def project_query(i, carry):
        rows = block(i, Q)
        qbuf[rows, :] = nn(normed[rows, :], query_w[...]).astype(BF16)
        return carry

    lax.fori_loop(0, 4, project_query, 0)

    a = jnp.where(is0, dec[0], dec[1])
    key_size = rqw.shape[1] // 2
    key_scale = key_size ** (-0.5)
    sub = lax.broadcasted_iota(jnp.int32, (C, 128), 0)
    trail = jnp.exp((C - 1.0 - sub.astype(F32)) * a) * key_scale
    turned = (rbuf[...].astype(F32) * trail).T
    t_high, t_low = split(turned)
    grown = nn(t_high, rbuf[...]) + nn(t_low, rbuf[...])
    lane16 = lax.broadcasted_iota(jnp.int32, (16, 128), 1)
    summ[z] = jnp.where(lane16 < 64, grown[96:112, :], pltpu.roll(grown[112:128, :], 64, 1))

    mx[...] = jnp.full_like(mx, LOW)
    tot[...] = jnp.zeros_like(tot)
    acc[...] = jnp.zeros_like(acc)
    fox_scale = (fqw.shape[1] // 2) ** (-0.5) * LOG2E
    R = C // 2

    def attend(i, js, masked):
        rows = block(i, R)
        query = qbuf[rows, :]
        blocks = [kv[block(j, C), :] for j in js]
        scores = [nt(query, b) * fox_scale + dall[:, block(j, C)] for j, b in zip(js, blocks)]
        if masked:
            q_at = lax.broadcasted_iota(jnp.int32, (R, C), 0) + i * R
            k_at = lax.broadcasted_iota(jnp.int32, (R, C), 1)
            scores = [jnp.where(k_at <= q_at, s, LOW) for s in scores]
        tops = [s[:, n * 128 : (n + 1) * 128] for s in scores for n in range(C // 128)]
        top = functools.reduce(jnp.maximum, tops)
        old = mx[rows, :]
        new = jnp.maximum(old, jnp.max(top, axis=1, keepdims=True))
        alpha = jnp.exp2(old - new)
        parts = [jnp.exp2(s - new) for s in tops]
        tot[rows, :] = alpha * tot[rows, :] + functools.reduce(jnp.add, parts)
        mx[rows, :] = new
        each = C // 128
        weighted = [
            nn(jnp.concatenate([p.astype(BF16) for p in parts[n * each : (n + 1) * each]], axis=1), b)
            for n, b in enumerate(blocks)
        ]
        acc[rows, :] = alpha * acc[rows, :] + functools.reduce(jnp.add, weighted)

    def inner(i):
        rows = block(i, Q)
        lanes = lax.broadcasted_iota(jnp.int32, (Q, 128), 1)
        query = jnp.where(jnp.logical_and(lanes >= 64, lanes < 96), rbuf[rows, :].astype(F32), 0.0).astype(BF16)
        keys = pltpu.roll(rbuf[...].astype(F32), 96, 1).astype(BF16)
        s = nt(query, keys)
        gap = lax.broadcasted_iota(jnp.int32, s.shape, 0) + i * Q - lax.broadcasted_iota(jnp.int32, s.shape, 1)
        within = jnp.where(gap >= 0, jnp.exp(jnp.maximum(gap, 0).astype(F32) * a), 0.0)
        high, low = split(s * key_scale * within)
        rin[rows, :] = nn(high, rbuf[...]) + nn(low, rbuf[...])

    def past(i, s):
        j = left_block(s)

        @pl.when(jnp.logical_and(z - s >= 0, j < 0))
        def _():
            attend(i, [z - s], False)

        @pl.when(j >= 0)
        def _():
            attend(i, [z - s, j], False)

    def attend_loop(s, carry):
        for k in range(4):
            kv_step(k, s)
            if k == 3:
                kv_step(4, s)
            idx = 4 * (s - 1) + k

            @pl.when(s == 1)
            def _():
                inner(k)

            if k % 2 == 1:
                @pl.when(s == 1)
                def _():
                    attend(k // 2, [z], True)

                @pl.when(s > 1)
                def _():
                    past(k // 2, s - 1)

            if k == 0:
                @pl.when(idx == H)
                def _():
                    ot_all[1]()

                @pl.when(idx == max(H, 2 * H - 4))
                def _():
                    ot_all[2]()

        return carry

    kv_start(4)
    lax.fori_loop(1, H + 1, attend_loop, 0)

    def last(i, carry):
        past(i, H)
        return carry

    lax.fori_loop(0, 2, last, 0)

    span = float(C)
    far = z.astype(F32) * span

    def gather_state(j, total):
        gap = (z - 1 - j).astype(F32) * span
        return total + jnp.exp(jnp.zeros((16, 128), F32) + gap * a) * summ[j]

    packed = lax.fori_loop(0, z, gather_state, jnp.zeros((16, 128), F32))
    both = jnp.concatenate([packed, pltpu.roll(packed, 64, 1)], axis=0)
    start = jnp.where(is0, state[0], state[1])
    start = jnp.concatenate([start, jnp.zeros_like(start)], axis=1)
    lane32 = lax.broadcasted_iota(jnp.int32, (32, 128), 1)
    entering = jnp.where(lane32 < 64, both, 0.0) + jnp.exp(jnp.zeros((32, 128), F32) + far * a) * start
    entering = jnp.concatenate([jnp.zeros((64, 128), F32), entering, jnp.zeros((32, 128), F32)], axis=0)
    e_high, e_low = split(entering)
    hn = hng[...]
    hn = jnp.where(is0, hn, pltpu.roll(hn, 64, 1))

    def finish(i, carry):
        rows = pl.ds(pl.multiple_of(i * Q, Q), Q)
        lanes = lax.broadcasted_iota(jnp.int32, (Q, 128), 1)
        place = (lax.broadcasted_iota(jnp.int32, (Q, 128), 0) + i * Q).astype(F32)
        leading = jnp.exp((place + 1.0) * a)
        query = rbuf[rows, :]
        raw = rin[rows, :] + (nn(query, e_high) + nn(query, e_low)) * leading
        raw = jnp.where(lanes < 64, raw, 0.0)
        center = jnp.where(lanes < 64, raw - jnp.sum(raw, axis=1, keepdims=True) * (1.0 / 64), 0.0)
        spread = jnp.sum(center * center, axis=1, keepdims=True) * (1.0 / 64)
        ret = center * lax.rsqrt(spread + EPS) * hn
        fox = acc[rows, :] / jnp.sum(tot[rows, :], axis=1, keepdims=True)
        mix[rows, :] = jnp.where(lanes < 64, ret, fox).astype(BF16)
        return carry

    lax.fori_loop(0, 4, finish, 0)

    def mix_rows(core, member):
        return mix.at[pl.ds(pl.multiple_of(core * T + member * out_rows, out_rows), out_rows), :]

    here = mixall.at[x, :, pl.ds(pl.multiple_of(c * 128, 128), 128)]
    mix_sends = [remote(mix_rows(1 - c, x), here, mix_s.at[0], mix_r.at[0], sib)]
    for r in range(1, X):
        member = lax.rem(x + r, X)
        mix_sends.append(remote(mix_rows(c, member), here, mix_s.at[2 * r - 1], mix_r.at[2 * r - 1], peers[r - 1]))
        mix_sends.append(remote(mix_rows(1 - c, member), here, mix_s.at[2 * r], mix_r.at[2 * r], cross[r - 1]))
    for copy in mix_sends:
        copy.start()
    mixall[x, :, pl.ds(pl.multiple_of(c * 128, 128), 128)] = mix[
        pl.ds(pl.multiple_of(c * T + x * out_rows, out_rows), out_rows), :
    ]
    ot_all[3]()
    for copy in mix_sends:
        copy.wait_recv()

    tile = 256

    def project_out(n, carry):
        cols = pl.ds(pl.multiple_of(n * tile, tile), tile)
        total = jnp.zeros((out_rows, tile), F32)
        for g in range(X):
            total = total + nt(mixall[g], ot[g, cols, :]).astype(BF16).astype(F32)
        out[:, cols] = total.astype(BF16)
        return carry

    lax.fori_loop(0, D // tile, project_out, 0)

    for copy in mix_sends:
        copy.wait_send()
    tok_all[4]()
    ot_all[4]()
    for way in range(2):
        for reach in range(2):
            for k in range(4):
                w_copy(way, k, reach, z, 0).wait_send()
    for k in range(5):
        kv_end(k)


def local(Z, X, tokens, norm_gain, rqw, rkw, rvw, fqw, fkw, fvw, decay, state, hng, gates, row, fow):
    T = tokens.shape[0]
    C = 2 * T
    D = norm_gain.shape[0]
    H = Z // 2
    vm = pl.BlockSpec(memory_space=pltpu.VMEM)
    dma = pltpu.SemaphoreType.DMA
    in_specs = [vm] * 14
    in_specs[8] = pl.BlockSpec(memory_space=pltpu.SMEM)
    return pl.pallas_call(
        functools.partial(kernel, Z, X),
        out_shape=jax.ShapeDtypeStruct((T // X, D), BF16),
        in_specs=in_specs,
        out_specs=vm,
        scratch_shapes=[
            pltpu.VMEM((D, 256), BF16),
            pltpu.VMEM((D, 128), BF16),
            pltpu.VMEM((D // 2, 128), BF16),
            pltpu.VMEM((D, 128), BF16),
            pltpu.VMEM((rqw.shape[0], 256), BF16),
            pltpu.VMEM((rqw.shape[0], 128), BF16),
            pltpu.VMEM((rqw.shape[0] // 2, 128), BF16),
            pltpu.VMEM((2, T, D), BF16),
            pltpu.VMEM((C, D), BF16),
            pltpu.VMEM((Z * C, 128), BF16),
            pltpu.VMEM((C, 128), BF16),
            pltpu.VMEM((C, 128), BF16),
            pltpu.VMEM((C, 128), F32),
            pltpu.VMEM((Z, 16, 128), F32),
            pltpu.VMEM((1, Z * C), F32),
            pltpu.VMEM((C, 128), F32),
            pltpu.VMEM((C, 128), F32),
            pltpu.VMEM((C, 128), F32),
            pltpu.VMEM((X, D, 256), BF16),
            pltpu.VMEM((C, 128), BF16),
            pltpu.VMEM((X, T // X, 256), BF16),
            dma((3,)), dma((3,)),
            dma((X - 1,)), dma((X - 1,)), dma((X,)), dma((X,)), dma,
            dma((2, 2, 4)), dma((2, 2, H // 2, 4)),
            dma((2, 5)), dma((H, 5)), dma((H - 1, 5)), pltpu.SemaphoreType.REGULAR,
            dma((X - 1,)), dma((X - 1,)), dma((X,)), dma((X,)), dma,
            dma((2 * X - 1,)), dma((2 * X - 1,)),
        ],
        compiler_params=pltpu.CompilerParams(
            collective_id=0, has_side_effects=True, vmem_limit_bytes=56 * 1024 * 1024
        ),
    )(
        tokens, norm_gain.reshape(1, -1), rqw, rkw, rvw, fqw, fkw, fvw, decay, state,
        hng.reshape(1, -1), gates.T, row.T, fow.T,
    )


def solution(mesh):
    Z, X = mesh.shape["sp"] // 2, mesh.shape["tp"]
    return jax.shard_map(
        functools.partial(local, Z, X),
        mesh=mesh,
        in_specs=(
            P(("grp", "sp"), "tp"),
            P(),
            P("sp", "tp"),
            P("sp", "tp"),
            P("sp", "tp"),
            P("sp", "tp"),
            P("sp", "tp"),
            P("sp", "tp"),
            P("tp"),
            P(("grp", "tp"), None, None),
            P("tp"),
            P("grp", "tp"),
            P("tp", "sp"),
            P("tp", "sp"),
        ),
        out_specs=P(("grp", "sp", "tp"), None),
        check_vma=False,
    )
```

time: 181 us -> 159 us (0.88)
  the two profiles are of different devices: /device:TPU:33 before, /device:TPU:1121 now
where the time goes in v2:
time: 159 us
  Pallas kernels  157 us (99%)
  local copies, waits for them, and re-layouts  1.67 us (1%)
    pallas_call x1, Pallas kernels, local(): pl.pallas_call(functools.partial(kernel, Z, X), out_shape=jax.ShapeDtypeS...  157 us

profile of v2, /device:TPU:1121, one launch (start us, length us, event | category | flops | bytes accessed | tf_op | source)
XLA Modules:
  0.0 158.9 jit_solution(836940432495210636)
XLA Ops:
  0.0 157.3 %shard_map.136 = bf16[64,2048]{1,0:T(8,128)(2,1)} custom-call(bf16[256,512]{1,0:T(8,128)(2,1)} %tok.1, f32[1,2048]{1,0:T(1,128)} %bitcast.6, bf16[32,64]{1,0:T(8,128)(2,1)} %rqw.1, bf16[32,64]{1,0:T(8,128)(2,1)} %rkw.1, bf16[32,128]{1,0:T(8,128)(2,1)} %rvw.1, bf16[32,128]{1,0:T(8,128)(2,1)} %fqw.1, bf16[32,128]{1,0:T(8,128)(2,1)} %fkw.1, ...), custom_call_target="tpu_custom_call" | custom-call | tf_op jit(solution)/shard_map/pallas_call | solution.py:562
  157.3 1.7 %copy.16 = bf16[64,2048]{1,0:T(8,128)(2,1)} copy(bf16[64,2048]{1,0:T(8,128)(2,1)} %shard_map.136) | data formatting | bytes 524288

commit v3 on v2

--- a/solution.py
+++ b/solution.py
@@ -271,6 +271,11 @@
         way = 0 if k < 2 else 1
         w_copy(way, k, 1, origin(way, H), last_t).wait_recv()
 
+    ot_all = row_gather(
+        out_w, lambda member: ot.at[member, :, block(c, 128)], ot_s, ot_r, otc_s, otc_r, ot_l
+    )
+    ot_all[0]()
+
     def project_wide(i, carry):
         rows = block(i, Q)
         both = nn(normed[rows, :], wide_w[...]).astype(BF16)
@@ -294,10 +299,6 @@
         def _():
             right_copy(k, z, 1).start()
 
-        @pl.when(early)
-        def _():
-            left_copy(k, jnp.minimum(z, H - 2), final).start()
-
     def left_block(s):
         return s - 2 - (Z - 1 - z)
 
@@ -337,17 +338,8 @@
         def _():
             left_copy(k, 0, final).wait_send()
 
-    @pl.when(early)
-    def _():
-        pl.semaphore_wait(ready, 1)
-
     for k in range(4):
         kv_start(k)
-
-    ot_all = row_gather(
-        out_w, lambda member: ot.at[member, :, block(c, 128)], ot_s, ot_r, otc_s, otc_r, ot_l
-    )
-    ot_all[0]()
 
     lane_p = lax.broadcasted_iota(jnp.int32, (rows_w, 128), 1) < 64
     half_w = rows_w // 2
@@ -433,18 +425,66 @@
         def _():
             attend(i, [z - s, j], False)
 
+    def finish_retention():
+        span = float(C)
+        far = z.astype(F32) * span
+
+        def gather_state(j, total):
+            gap = (z - 1 - j).astype(F32) * span
+            return total + jnp.exp(jnp.zeros((16, 128), F32) + gap * a) * summ[j]
+
+        packed = lax.fori_loop(0, z, gather_state, jnp.zeros((16, 128), F32))
+        both = jnp.concatenate([packed, pltpu.roll(packed, 64, 1)], axis=0)
+        start = jnp.where(is0, state[0], state[1])
+        start = jnp.concatenate([start, jnp.zeros_like(start)], axis=1)
+        lane32 = lax.broadcasted_iota(jnp.int32, (32, 128), 1)
+        entering = jnp.where(lane32 < 64, both, 0.0) + jnp.exp(jnp.zeros((32, 128), F32) + far * a) * start
+        entering = jnp.concatenate([jnp.zeros((64, 128), F32), entering, jnp.zeros((32, 128), F32)], axis=0)
+        e_high, e_low = split(entering)
+        hn = hng[...]
+        hn = jnp.where(is0, hn, pltpu.roll(hn, 64, 1))
+
+        def piece(i, carry):
+            rows = block(i, Q)
+            lanes = lax.broadcasted_iota(jnp.int32, (Q, 128), 1)
+            place = (lax.broadcasted_iota(jnp.int32, (Q, 128), 0) + i * Q).astype(F32)
+            leading = jnp.exp((place + 1.0) * a)
+            query = rbuf[rows, :]
+            raw = rin[rows, :] + (nn(query, e_high) + nn(query, e_low)) * leading
+            raw = jnp.where(lanes < 64, raw, 0.0)
+            center = jnp.where(lanes < 64, raw - jnp.sum(raw, axis=1, keepdims=True) * (1.0 / 64), 0.0)
+            spread = jnp.sum(center * center, axis=1, keepdims=True) * (1.0 / 64)
+            rin[rows, :] = center * lax.rsqrt(spread + EPS) * hn
+            return carry
+
+        lax.fori_loop(0, 4, piece, 0)
+
+    def send_far(s):
+        @pl.when(jnp.logical_and(early, s == (3 * z + 2) // 4 + 1))
+        def _():
+            pl.semaphore_wait(ready, 1)
+            for k in (4, 0, 1, 2, 3):
+                left_copy(k, jnp.minimum(z, H - 2), final).start()
+
     def attend_loop(s, carry):
+        send_far(s)
+        kv_step(4, s)
         for k in range(4):
             kv_step(k, s)
-            if k == 3:
-                kv_step(4, s)
             idx = 4 * (s - 1) + k
 
             @pl.when(s == 1)
             def _():
                 inner(k)
 
+            if k == 0:
+
+                @pl.when(s == H)
+                def _():
+                    finish_retention()
+
             if k % 2 == 1:
+
                 @pl.when(s == 1)
                 def _():
                     attend(k // 2, [z], True)
@@ -473,37 +513,11 @@
 
     lax.fori_loop(0, 2, last, 0)
 
-    span = float(C)
-    far = z.astype(F32) * span
-
-    def gather_state(j, total):
-        gap = (z - 1 - j).astype(F32) * span
-        return total + jnp.exp(jnp.zeros((16, 128), F32) + gap * a) * summ[j]
-
-    packed = lax.fori_loop(0, z, gather_state, jnp.zeros((16, 128), F32))
-    both = jnp.concatenate([packed, pltpu.roll(packed, 64, 1)], axis=0)
-    start = jnp.where(is0, state[0], state[1])
-    start = jnp.concatenate([start, jnp.zeros_like(start)], axis=1)
-    lane32 = lax.broadcasted_iota(jnp.int32, (32, 128), 1)
-    entering = jnp.where(lane32 < 64, both, 0.0) + jnp.exp(jnp.zeros((32, 128), F32) + far * a) * start
-    entering = jnp.concatenate([jnp.zeros((64, 128), F32), entering, jnp.zeros((32, 128), F32)], axis=0)
-    e_high, e_low = split(entering)
-    hn = hng[...]
-    hn = jnp.where(is0, hn, pltpu.roll(hn, 64, 1))
-
     def finish(i, carry):
-        rows = pl.ds(pl.multiple_of(i * Q, Q), Q)
+        rows = block(i, Q)
         lanes = lax.broadcasted_iota(jnp.int32, (Q, 128), 1)
-        place = (lax.broadcasted_iota(jnp.int32, (Q, 128), 0) + i * Q).astype(F32)
-        leading = jnp.exp((place + 1.0) * a)
-        query = rbuf[rows, :]
-        raw = rin[rows, :] + (nn(query, e_high) + nn(query, e_low)) * leading
-        raw = jnp.where(lanes < 64, raw, 0.0)
-        center = jnp.where(lanes < 64, raw - jnp.sum(raw, axis=1, keepdims=True) * (1.0 / 64), 0.0)
-        spread = jnp.sum(center * center, axis=1, keepdims=True) * (1.0 / 64)
-        ret = center * lax.rsqrt(spread + EPS) * hn
         fox = acc[rows, :] / jnp.sum(tot[rows, :], axis=1, keepdims=True)
-        mix[rows, :] = jnp.where(lanes < 64, ret, fox).astype(BF16)
+        mix[rows, :] = jnp.where(lanes < 64, rin[rows, :], fox).astype(BF16)
         return carry
 
     lax.fori_loop(0, 4, finish, 0)

time: 159 us -> 151 us (0.950)
  the two profiles are of different devices: /device:TPU:1121 before, /device:TPU:1185 now
where the time goes in v3:
time: 151 us; the launch traced here: 150 us
  Pallas kernels  149 us (99%)
  local copies, waits for them, and re-layouts  1.67 us (1%)
    pallas_call x1, Pallas kernels, local(): pl.pallas_call(functools.partial(kernel, Z, X), out_shape=jax.ShapeDtypeS...  149 us

profile of v3, /device:TPU:1185, one launch (start us, length us, event | category | flops | bytes accessed | tf_op | source)
XLA Modules:
  0.0 150.5 jit_solution(8956091216200721244)
XLA Ops:
  0.0 148.8 %shard_map.136 = bf16[64,2048]{1,0:T(8,128)(2,1)} custom-call(bf16[256,512]{1,0:T(8,128)(2,1)} %tok.1, f32[1,2048]{1,0:T(1,128)} %bitcast.6, bf16[32,64]{1,0:T(8,128)(2,1)} %rqw.1, bf16[32,64]{1,0:T(8,128)(2,1)} %rkw.1, bf16[32,128]{1,0:T(8,128)(2,1)} %rvw.1, bf16[32,128]{1,0:T(8,128)(2,1)} %fqw.1, bf16[32,128]{1,0:T(8,128)(2,1)} %fkw.1, ...), custom_call_target="tpu_custom_call" | custom-call | tf_op jit(solution)/shard_map/pallas_call | solution.py:576
  148.8 1.7 %copy.16 = bf16[64,2048]{1,0:T(8,128)(2,1)} copy(bf16[64,2048]{1,0:T(8,128)(2,1)} %shard_map.136) | data formatting | bytes 524288

commit v4 on v3

--- a/solution.py
+++ b/solution.py
@@ -179,8 +179,8 @@
         if k < 2:
             return wide_w.at[block(2 * o + k, rows_w), :]
         if k == 2:
-            return out_w.at[block(o, chip_w), :]
-        return pack_w.at[block(o, rows_w), :]
+            return pack_w.at[block(o, rows_w), :]
+        return out_w.at[block(o, chip_w), :]
 
     def origin(way, d):
         return lax.rem(z - d + Z, Z) if way == 0 else lax.rem(z + d, Z)
@@ -260,21 +260,19 @@
     for p in range(inside, pieces):
         normalize(jnp.int32(p))
 
-    def weights_end(t, carry):
-        for k in range(4):
-            for way in range(2):
-                w_copy(way, k, 0, origin(way, 2 * t + 1), t).wait_recv()
-        return carry
-
-    lax.fori_loop(0, rounds, weights_end, 0)
-    for k in range(4):
-        way = 0 if k < 2 else 1
-        w_copy(way, k, 1, origin(way, H), last_t).wait_recv()
-
-    ot_all = row_gather(
-        out_w, lambda member: ot.at[member, :, block(c, 128)], ot_s, ot_r, otc_s, otc_r, ot_l
-    )
-    ot_all[0]()
+    def weights_end(chunks):
+        def body(t, carry):
+            for k in chunks:
+                for way in range(2):
+                    w_copy(way, k, 0, origin(way, 2 * t + 1), t).wait_recv()
+            return carry
+
+        lax.fori_loop(0, rounds, body, 0)
+        for k in chunks:
+            way = 0 if k < 2 else 1
+            w_copy(way, k, 1, origin(way, H), last_t).wait_recv()
+
+    weights_end((0, 1))
 
     def project_wide(i, carry):
         rows = block(i, Q)
@@ -285,8 +283,10 @@
 
     lax.fori_loop(0, 4, project_wide, 0)
 
+    NK = 8
+
     def kv_at(k, o):
-        return kv.at[block(o * 4 + k, Q), :] if k < 4 else summ.at[o]
+        return kv.at[block(o * NK + k, C // NK), :] if k < NK else summ.at[o]
 
     def right_copy(k, o, s):
         return remote(kv_at(k, o), kv_at(k, o), ks.at[0, k], kr.at[s - 1, k], hops[0][0])
@@ -299,11 +299,11 @@
         def _():
             right_copy(k, z, 1).start()
 
-    def left_block(s):
-        return s - 2 - (Z - 1 - z)
+    def left_block(s, lag=4):
+        return s - lag - (Z - 1 - z)
 
     def kv_step(k, s):
-        @pl.when(z - s >= 0)
+        @pl.when(jnp.logical_and(z - s >= 0, s <= H))
         def _():
             o = z - s
             right_copy(k, o, s).wait_recv()
@@ -314,7 +314,7 @@
                 nxt.wait_send()
                 nxt.start()
 
-        j = left_block(s)
+        j = left_block(s, 4 if k < NK else 2)
 
         @pl.when(j >= 0)
         def _():
@@ -338,8 +338,14 @@
         def _():
             left_copy(k, 0, final).wait_send()
 
-    for k in range(4):
+    for k in range(NK):
         kv_start(k)
+
+    weights_end((2, 3))
+    ot_all = row_gather(
+        out_w, lambda member: ot.at[member, :, block(c, 128)], ot_s, ot_r, otc_s, otc_r, ot_l
+    )
+    ot_all[0]()
 
     lane_p = lax.broadcasted_iota(jnp.int32, (rows_w, 128), 1) < 64
     half_w = rows_w // 2
@@ -417,13 +423,19 @@
     def past(i, s):
         j = left_block(s)
 
-        @pl.when(jnp.logical_and(z - s >= 0, j < 0))
+        right_too = jnp.logical_and(z - s >= 0, s <= H)
+
+        @pl.when(jnp.logical_and(right_too, j < 0))
         def _():
             attend(i, [z - s], False)
 
-        @pl.when(j >= 0)
+        @pl.when(jnp.logical_and(right_too, j >= 0))
         def _():
             attend(i, [z - s, j], False)
+
+        @pl.when(jnp.logical_and(j >= 0, s > H))
+        def _():
+            attend(i, [j], False)
 
     def finish_retention():
         span = float(C)
@@ -459,23 +471,29 @@
 
         lax.fori_loop(0, 4, piece, 0)
 
-    def send_far(s):
-        @pl.when(jnp.logical_and(early, s == (3 * z + 2) // 4 + 1))
-        def _():
-            pl.semaphore_wait(ready, 1)
-            for k in (4, 0, 1, 2, 3):
-                left_copy(k, jnp.minimum(z, H - 2), final).start()
+    def send_far(ks_now):
+        for k in ks_now:
+            left_copy(k, jnp.minimum(z, H - 2), final).start()
+
+    pace = (29 * z) // 4 + jnp.where(z > 0, NK // 2, 0)
 
     def attend_loop(s, carry):
-        send_far(s)
-        kv_step(4, s)
-        for k in range(4):
+        @pl.when(s <= H)
+        def _():
+            kv_step(NK, s)
+
+        for k in range(NK):
             kv_step(k, s)
-            idx = 4 * (s - 1) + k
-
-            @pl.when(s == 1)
+
+            @pl.when(jnp.logical_and(early, NK * (s - 1) + k == pace))
             def _():
-                inner(k)
+                send_far(range(NK))
+
+            if k % 2 == 0:
+
+                @pl.when(s == 1)
+                def _():
+                    inner(k // 2)
 
             if k == 0:
 
@@ -483,35 +501,43 @@
                 def _():
                     finish_retention()
 
-            if k % 2 == 1:
+                @pl.when(s == H // 4 + 1)
+                def _():
+                    ot_all[1]()
+
+                @pl.when(s == max(H // 4 + 1, H // 2))
+                def _():
+                    ot_all[2]()
+
+            if k % 4 == 3:
 
                 @pl.when(s == 1)
                 def _():
-                    attend(k // 2, [z], True)
+                    attend(k // 4, [z], True)
 
                 @pl.when(s > 1)
                 def _():
-                    past(k // 2, s - 1)
-
-            if k == 0:
-                @pl.when(idx == H)
-                def _():
-                    ot_all[1]()
-
-                @pl.when(idx == max(H, 2 * H - 4))
-                def _():
-                    ot_all[2]()
+                    past(k // 4, s - 1)
 
         return carry
 
-    kv_start(4)
-    lax.fori_loop(1, H + 1, attend_loop, 0)
-
-    def last(i, carry):
-        past(i, H)
-        return carry
-
-    lax.fori_loop(0, 2, last, 0)
+    kv_start(NK)
+
+    @pl.when(early)
+    def _():
+        pl.semaphore_wait(ready, 1)
+        send_far([NK])
+
+    lax.fori_loop(1, H + 3, attend_loop, 0)
+
+    @pl.when(left_block(H + 2) >= 0)
+    def _():
+        def last(i, carry):
+            attend(i, [left_block(H + 2)], False)
+            return carry
+
+        lax.fori_loop(0, 2, last, 0)
+
 
     def finish(i, carry):
         rows = block(i, Q)
@@ -560,7 +586,7 @@
         for reach in range(2):
             for k in range(4):
                 w_copy(way, k, reach, z, 0).wait_send()
-    for k in range(5):
+    for k in range(NK + 1):
         kv_end(k)
 
 
@@ -603,7 +629,7 @@
             dma((3,)), dma((3,)),
             dma((X - 1,)), dma((X - 1,)), dma((X,)), dma((X,)), dma,
             dma((2, 2, 4)), dma((2, 2, H // 2, 4)),
-            dma((2, 5)), dma((H, 5)), dma((H - 1, 5)), pltpu.SemaphoreType.REGULAR,
+            dma((2, 9)), dma((H, 9)), dma((H - 1, 9)), pltpu.SemaphoreType.REGULAR,
             dma((X - 1,)), dma((X - 1,)), dma((X,)), dma((X,)), dma,
             dma((2 * X - 1,)), dma((2 * X - 1,)),
         ],

time: 151 us -> 129 us (0.85)
  the two profiles are of different devices: /device:TPU:1185 before, /device:TPU:1129 now
where the time goes in v4:
time: 129 us
  Pallas kernels  127 us (98%)
  local copies, waits for them, and re-layouts  1.67 us (1%)
    pallas_call x1, Pallas kernels, local(): pl.pallas_call(functools.partial(kernel, Z, X), out_shape=jax.ShapeDtypeS...  127 us

profile of v4, /device:TPU:1129, one launch (start us, length us, event | category | flops | bytes accessed | tf_op | source)
XLA Modules:
  0.0 128.7 jit_solution(14719624125729230931)
XLA Ops:
  0.0 127.0 %shard_map.136 = bf16[64,2048]{1,0:T(8,128)(2,1)} custom-call(bf16[256,512]{1,0:T(8,128)(2,1)} %tok.1, f32[1,2048]{1,0:T(1,128)} %bitcast.6, bf16[32,64]{1,0:T(8,128)(2,1)} %rqw.1, bf16[32,64]{1,0:T(8,128)(2,1)} %rkw.1, bf16[32,128]{1,0:T(8,128)(2,1)} %rvw.1, bf16[32,128]{1,0:T(8,128)(2,1)} %fqw.1, bf16[32,128]{1,0:T(8,128)(2,1)} %fkw.1, ...), custom_call_target="tpu_custom_call" | custom-call | tf_op jit(solution)/shard_map/pallas_call | solution.py:602
  127.0 1.7 %copy.16 = bf16[64,2048]{1,0:T(8,128)(2,1)} copy(bf16[64,2048]{1,0:T(8,128)(2,1)} %shard_map.136) | data formatting | bytes 524288

commit v5 on v4

--- a/solution.py
+++ b/solution.py
@@ -299,7 +299,7 @@
         def _():
             right_copy(k, z, 1).start()
 
-    def left_block(s, lag=4):
+    def left_block(s, lag=3):
         return s - lag - (Z - 1 - z)
 
     def kv_step(k, s):
@@ -314,7 +314,7 @@
                 nxt.wait_send()
                 nxt.start()
 
-        j = left_block(s, 4 if k < NK else 2)
+        j = left_block(s, 3 if k < NK else 2)
 
         @pl.when(j >= 0)
         def _():
@@ -433,10 +433,6 @@
         def _():
             attend(i, [z - s, j], False)
 
-        @pl.when(jnp.logical_and(j >= 0, s > H))
-        def _():
-            attend(i, [j], False)
-
     def finish_retention():
         span = float(C)
         far = z.astype(F32) * span
@@ -482,6 +478,10 @@
         def _():
             kv_step(NK, s)
 
+        @pl.when(s == H + 1)
+        def _():
+            finish_retention()
+
         for k in range(NK):
             kv_step(k, s)
 
@@ -496,10 +496,6 @@
                     inner(k // 2)
 
             if k == 0:
-
-                @pl.when(s == H)
-                def _():
-                    finish_retention()
 
                 @pl.when(s == H // 4 + 1)
                 def _():
@@ -528,15 +524,15 @@
         pl.semaphore_wait(ready, 1)
         send_far([NK])
 
-    lax.fori_loop(1, H + 3, attend_loop, 0)
-
-    @pl.when(left_block(H + 2) >= 0)
+    lax.fori_loop(1, H + 2, attend_loop, 0)
+
+    @pl.when(left_block(H + 1) >= 0)
     def _():
         def last(i, carry):
-            attend(i, [left_block(H + 2)], False)
+            attend(i, [left_block(H + 1)], False)
             return carry
 
-        lax.fori_loop(0, 2, last, 0)
+        lax.fori_loop(0, 2, last, 0, unroll=2)
 
 
     def finish(i, carry):
@@ -576,7 +572,7 @@
         out[:, cols] = total.astype(BF16)
         return carry
 
-    lax.fori_loop(0, D // tile, project_out, 0)
+    lax.fori_loop(0, D // tile, project_out, 0, unroll=2)
 
     for copy in mix_sends:
         copy.wait_send()

time: 129 us -> 124 us (0.961)
  the two profiles are of different devices: /device:TPU:1129 before, /device:TPU:1121 now
where the time goes in v5:
time: 124 us
  Pallas kernels  122 us (98%)
  local copies, waits for them, and re-layouts  1.67 us (1%)
    pallas_call x1, Pallas kernels, local(): pl.pallas_call(functools.partial(kernel, Z, X), out_shape=jax.ShapeDtypeS...  122 us

profile of v5, /device:TPU:1121, one launch (start us, length us, event | category | flops | bytes accessed | tf_op | source)
XLA Modules:
  0.0 124.0 jit_solution(17989566408835114669)
XLA Ops:
  0.0 122.4 %shard_map.136 = bf16[64,2048]{1,0:T(8,128)(2,1)} custom-call(bf16[256,512]{1,0:T(8,128)(2,1)} %tok.1, f32[1,2048]{1,0:T(1,128)} %bitcast.6, bf16[32,64]{1,0:T(8,128)(2,1)} %rqw.1, bf16[32,64]{1,0:T(8,128)(2,1)} %rkw.1, bf16[32,128]{1,0:T(8,128)(2,1)} %rvw.1, bf16[32,128]{1,0:T(8,128)(2,1)} %fqw.1, bf16[32,128]{1,0:T(8,128)(2,1)} %fkw.1, ...), custom_call_target="tpu_custom_call" | custom-call | tf_op jit(solution)/shard_map/pallas_call | solution.py:598
  122.4 1.7 %copy.16 = bf16[64,2048]{1,0:T(8,128)(2,1)} copy(bf16[64,2048]{1,0:T(8,128)(2,1)} %shard_map.136) | data formatting | bytes 524288

commit v6 on v5

--- a/solution.py
+++ b/solution.py
@@ -35,11 +35,14 @@
     out,
     wide_w, out_w, pack_w, query_w, send_w, send_o, send_p,
     tokall, normed, kv, qbuf, rbuf, rin, summ, dall, mx, tot, acc, ot, mix, mixall,
-    swap_s, swap_r, tok_s, tok_r, tokc_s, tokc_r, tok_l, ws, wr, ks, kr, kl, ready,
+    swap_s, swap_r, tok_s, tok_r, tokc_s, tokc_r, tok_l, ws, wr, ys, yr, ks, kr, kl, ready,
     ot_s, ot_r, otc_s, otc_r, ot_l, mix_s, mix_r,
 ):
     sp = lax.axis_index("sp")
     x = lax.axis_index("tp")
+    grp = lax.axis_index("grp")
+    part = lax.rem(grp, 2)
+    pair = {"grp": grp + 1 - 2 * part}
     c = lax.rem(sp, 2)
     z = sp // 2
     H = Z // 2
@@ -93,7 +96,7 @@
     send_p[...] = jnp.where(is0, second[2], first[2]).astype(BF16)
 
     barrier = pltpu.get_barrier_semaphore()
-    partners = [hops[0][0], hops[0][1], hops[1][0], hops[1][1], sib] + peers + cross
+    partners = [hops[0][0], hops[0][1], hops[1][0], hops[1][1], sib, pair] + peers + cross
     for dev in partners:
         pl.semaphore_signal(barrier, inc=1, device_id=dev, device_id_type=MESH)
     early = z <= H - 2
@@ -175,20 +178,33 @@
     for copy in swaps:
         copy.wait()
 
-    def w_at(k, o):
-        if k < 2:
-            return wide_w.at[block(2 * o + k, rows_w), :]
-        if k == 2:
-            return pack_w.at[block(o, rows_w), :]
-        return out_w.at[block(o, chip_w), :]
+    def w_at(k, o, half):
+        if k == 0:
+            return wide_w.at[block(2 * o + half, rows_w), :]
+        if k == 1:
+            return out_w.at[block(2 * o + half, rows_w), :]
+        return pack_w.at[block(2 * o + half, rows_w // 2), :]
 
     def origin(way, d):
         return lax.rem(z - d + Z, Z) if way == 0 else lax.rem(z + d, Z)
 
     def w_copy(way, k, reach, o, t):
-        return remote(
-            w_at(k, o), w_at(k, o), ws.at[way, reach, k], wr.at[way, reach, t, k], hops[way][reach]
-        )
+        where = w_at(k, o, part)
+        return remote(where, where, ws.at[way, reach, k], wr.at[way, reach, t, k], hops[way][reach])
+
+    def y_copy(way, k, reach, t, half):
+        where = w_at(k, origin(way, 2 * t + 1 + reach), half)
+        return remote(where, where, ys.at[way, reach, k], yr.at[way, reach, t, k], pair)
+
+    def hand_over(way, k, reach, t):
+        w_copy(way, k, reach, origin(way, 2 * t + 1 + reach), t).wait_recv()
+        copy = y_copy(way, k, reach, t, part)
+
+        @pl.when(t > 0)
+        def _():
+            copy.wait_send()
+
+        copy.start()
 
     last_t = H // 2 - 1
 
@@ -202,7 +218,6 @@
                 w_copy(way, k, 0, o, t).wait_send()
 
             w_copy(way, k, 0, o, t).start()
-            mine = (k < 2) == (way == 0)
 
             def pass_two(way=way, o=o):
                 @pl.when(t > 0)
@@ -211,18 +226,27 @@
 
                 w_copy(way, k, 1, o, t).start()
 
-            if mine:
+            if (k < 1) == (way == 0):
                 pass_two()
             else:
                 pl.when(t < last_t)(pass_two)
 
+        @pl.when(t > 0)
+        def _():
+            for way in range(2):
+                copy = y_copy(way, k, 1, t - 1, part)
+
+                @pl.when(t > 1)
+                def _(copy=copy):
+                    copy.wait_send()
+
+                copy.start()
+                hand_over(way, k, 0, t - 1)
+
     pieces = 8
     P_rows = C // pieces
     rounds = last_t + 1
-    w_total = 4 * rounds
-    base = w_total // 2 + 1
-    stride = 2
-    inside = min(pieces, (w_total - base + stride - 1) // stride)
+    inside = 2 * (rounds - rounds // 2)
 
     def normalize(p):
         @pl.when(p == pieces // 2)
@@ -236,43 +260,54 @@
         normed[block(at, P_rows), :] = (values * scale * gain[...]).astype(BF16)
 
     def weights_loop(t, carry):
-        for k in range(4):
+        for k in range(3):
             w_step(t, k)
-            idx = 4 * t + k
-
-            @pl.when(idx == w_total // 4)
-            def _():
-                tok_all[1]()
-
-            @pl.when(idx == w_total // 2)
-            def _():
-                tok_all[2]()
-
-            if k % 2 == 1:
-
-                @pl.when(jnp.logical_and(idx >= base, idx < base + stride * inside))
-                def _():
-                    normalize((idx - base) // stride)
+            if k == 0:
+
+                @pl.when(t == rounds // 4)
+                def _():
+                    tok_all[1]()
+
+                @pl.when(t == rounds // 2)
+                def _():
+                    tok_all[2]()
+
+            if k < 2:
+
+                @pl.when(t >= rounds // 2)
+                def _():
+                    normalize(2 * (t - rounds // 2) + k)
 
         return carry
 
     lax.fori_loop(0, rounds, weights_loop, 0)
+
+    def weights_end(k):
+        mine = 0 if k < 1 else 1
+        for way in range(2):
+            hand_over(way, k, 0, jnp.int32(last_t))
+        hand_over(mine, k, 1, jnp.int32(last_t))
+
+    def weights_here(k):
+        mine = 0 if k < 1 else 1
+
+        def body(t, carry):
+            for way in range(2):
+                y_copy(way, k, 0, t, 1 - part).wait_recv()
+
+                @pl.when(jnp.logical_or(t < last_t, way == mine))
+                def _(way=way):
+                    y_copy(way, k, 1, t, 1 - part).wait_recv()
+
+            return carry
+
+        lax.fori_loop(0, rounds, body, 0)
+
+    for k in range(3):
+        weights_end(k)
     for p in range(inside, pieces):
         normalize(jnp.int32(p))
-
-    def weights_end(chunks):
-        def body(t, carry):
-            for k in chunks:
-                for way in range(2):
-                    w_copy(way, k, 0, origin(way, 2 * t + 1), t).wait_recv()
-            return carry
-
-        lax.fori_loop(0, rounds, body, 0)
-        for k in chunks:
-            way = 0 if k < 2 else 1
-            w_copy(way, k, 1, origin(way, H), last_t).wait_recv()
-
-    weights_end((0, 1))
+    weights_here(0)
 
     def project_wide(i, carry):
         rows = block(i, Q)
@@ -341,11 +376,13 @@
     for k in range(NK):
         kv_start(k)
 
-    weights_end((2, 3))
+    weights_here(1)
     ot_all = row_gather(
         out_w, lambda member: ot.at[member, :, block(c, 128)], ot_s, ot_r, otc_s, otc_r, ot_l
     )
     ot_all[0]()
+
+    weights_here(2)
 
     lane_p = lax.broadcasted_iota(jnp.int32, (rows_w, 128), 1) < 64
     half_w = rows_w // 2
@@ -580,8 +617,9 @@
     ot_all[4]()
     for way in range(2):
         for reach in range(2):
-            for k in range(4):
+            for k in range(3):
                 w_copy(way, k, reach, z, 0).wait_send()
+                y_copy(way, k, reach, 0, part).wait_send()
     for k in range(NK + 1):
         kv_end(k)
 
@@ -624,7 +662,7 @@
             pltpu.VMEM((X, T // X, 256), BF16),
             dma((3,)), dma((3,)),
             dma((X - 1,)), dma((X - 1,)), dma((X,)), dma((X,)), dma,
-            dma((2, 2, 4)), dma((2, 2, H // 2, 4)),
+            dma((2, 2, 3)), dma((2, 2, H // 2, 3)), dma((2, 2, 3)), dma((2, 2, H // 2, 3)),
             dma((2, 9)), dma((H, 9)), dma((H - 1, 9)), pltpu.SemaphoreType.REGULAR,
             dma((X - 1,)), dma((X - 1,)), dma((X,)), dma((X,)), dma,
             dma((2 * X - 1,)), dma((2 * X - 1,)),

time: 124 us -> 126 us (1.016)
  Pallas kernels: 122 us -> 124 us
    pallas_call x1, Pallas kernels: 122 us -> 124 us  [local(): pl.pallas_call(functools.partial(kernel, Z, X), out_shape=jax.ShapeDtypeS...]
where the time goes in v6:
time: 126 us
  Pallas kernels  124 us (98%)
  local copies, waits for them, and re-layouts  1.67 us (1%)
    pallas_call x1, Pallas kernels, local(): pl.pallas_call(functools.partial(kernel, Z, X), out_shape=jax.ShapeDtypeS...  124 us

profile of v6, /device:TPU:1121, one launch (start us, length us, event | category | flops | bytes accessed | tf_op | source)
XLA Modules:
  0.0 125.6 jit_solution(6581191264794444600)
XLA Ops:
  0.0 123.9 %shard_map.136 = bf16[64,2048]{1,0:T(8,128)(2,1)} custom-call(bf16[256,512]{1,0:T(8,128)(2,1)} %tok.1, f32[1,2048]{1,0:T(1,128)} %bitcast.6, bf16[32,64]{1,0:T(8,128)(2,1)} %rqw.1, bf16[32,64]{1,0:T(8,128)(2,1)} %rkw.1, bf16[32,128]{1,0:T(8,128)(2,1)} %rvw.1, bf16[32,128]{1,0:T(8,128)(2,1)} %fqw.1, bf16[32,128]{1,0:T(8,128)(2,1)} %fkw.1, ...), custom_call_target="tpu_custom_call" | custom-call | tf_op jit(solution)/shard_map/pallas_call | solution.py:636
  123.9 1.7 %copy.16 = bf16[64,2048]{1,0:T(8,128)(2,1)} copy(bf16[64,2048]{1,0:T(8,128)(2,1)} %shard_map.136) | data formatting | bytes 524288

commit v7 on v5

--- a/solution.py
+++ b/solution.py
@@ -281,7 +281,7 @@
         rbuf[rows, :] = both[:, 128:]
         return carry
 
-    lax.fori_loop(0, 4, project_wide, 0)
+    lax.fori_loop(0, 4, project_wide, 0, unroll=2)
 
     NK = 8
 
@@ -366,7 +366,7 @@
         qbuf[rows, :] = nn(normed[rows, :], query_w[...]).astype(BF16)
         return carry
 
-    lax.fori_loop(0, 4, project_query, 0)
+    lax.fori_loop(0, 4, project_query, 0, unroll=2)
 
     a = jnp.where(is0, dec[0], dec[1])
     key_size = rqw.shape[1] // 2
@@ -465,7 +465,7 @@
             rin[rows, :] = center * lax.rsqrt(spread + EPS) * hn
             return carry
 
-        lax.fori_loop(0, 4, piece, 0)
+        lax.fori_loop(0, 4, piece, 0, unroll=2)
 
     def send_far(ks_now):
         for k in ks_now:
@@ -542,7 +542,7 @@
         mix[rows, :] = jnp.where(lanes < 64, rin[rows, :], fox).astype(BF16)
         return carry
 
-    lax.fori_loop(0, 4, finish, 0)
+    lax.fori_loop(0, 4, finish, 0, unroll=2)
 
     def mix_rows(core, member):
         return mix.at[pl.ds(pl.multiple_of(core * T + member * out_rows, out_rows), out_rows), :]
@@ -572,7 +572,7 @@
         out[:, cols] = total.astype(BF16)
         return carry
 
-    lax.fori_loop(0, D // tile, project_out, 0, unroll=2)
+    lax.fori_loop(0, D // tile, project_out, 0, unroll=4)
 
     for copy in mix_sends:
         copy.wait_send()

time: 124 us -> 124 us (level)
  no operation moved by 1% of the time
where the time goes in v7:
time: 124 us; the launch traced here: 123 us
  Pallas kernels  122 us (98%)
  local copies, waits for them, and re-layouts  1.67 us (1%)
    pallas_call x1, Pallas kernels, local(): pl.pallas_call(functools.partial(kernel, Z, X), out_shape=jax.ShapeDtypeS...  122 us

profile of v7, /device:TPU:1121, one launch (start us, length us, event | category | flops | bytes accessed | tf_op | source)
XLA Modules:
  0.0 123.4 jit_solution(17762851643099022728)
XLA Ops:
  0.0 121.7 %shard_map.136 = bf16[64,2048]{1,0:T(8,128)(2,1)} custom-call(bf16[256,512]{1,0:T(8,128)(2,1)} %tok.1, f32[1,2048]{1,0:T(1,128)} %bitcast.6, bf16[32,64]{1,0:T(8,128)(2,1)} %rqw.1, bf16[32,64]{1,0:T(8,128)(2,1)} %rkw.1, bf16[32,128]{1,0:T(8,128)(2,1)} %rvw.1, bf16[32,128]{1,0:T(8,128)(2,1)} %fqw.1, bf16[32,128]{1,0:T(8,128)(2,1)} %fkw.1, ...), custom_call_target="tpu_custom_call" | custom-call | tf_op jit(solution)/shard_map/pallas_call | solution.py:598
  121.7 1.7 %copy.16 = bf16[64,2048]{1,0:T(8,128)(2,1)} copy(bf16[64,2048]{1,0:T(8,128)(2,1)} %shard_map.136) | data formatting | bytes 524288
